TPU v7x, 32 devices: a whole 2x2x4 slice. The times are simulated.
32 devices in a mesh: fs: 8 (over z, x), tp: 4 (over y, core).
Axes of the slice: x: 2, y: 2, z: 4, core: 2. Of those that a mesh axis runs over, the one named last changes fastest.
Arguments:
- inputs: bfloat16 [3072, 2048], P('fs'), may hold values from -6 to 6
- queries: bfloat16 [3072, 2048], P('fs', 'tp'), may hold values from -6 to 6
- keys: bfloat16 [3072, 2048], P('fs', 'tp'), may hold values from -6 to 6
- values: bfloat16 [3072, 2048], P('fs', 'tp'), may hold values from -6 to 6
- head_cot: bfloat16 [3072, 2048], P('fs', 'tp'), may hold values from -6 to 6
- mixing: float32 [16], P('tp'), may hold values from 0.3 to 0.8
- head_gain: float32 [128], replicated, may hold values from 0.1 to 1.9
- factors: bfloat16 [2048, 2, 256], P('fs'), may hold values from -0.375 to 0.375
- moments: float32 [256, 2, 2048], P('fs', None, 'tp'), may hold values from -6 to 6
- weights: float32 [2048, 2, 2048], P('fs', None, 'tp'), may hold values from -6 to 6
Outputs:
- step: float32 [2048, 2, 2048], P('fs', None, 'tp')
- new_moments: float32 [256, 2, 2048], P('fs', None, 'tp')
- copies: bfloat16 [2048, 2, 2048], P(None, None, 'tp')
All inputs are finite; a program needn't handle non-finite values.
Results may differ from a plain program's by a relative error of at most 0.007.
Values may be sent and summed in bfloat16 or wider, within the bound.
A program may use at most 64 MiB of HBM per device.

v0:
```python
import functools

import jax
import jax.numpy as jnp
from jax import lax
from jax.experimental import pallas as pl
from jax.experimental.pallas import tpu as pltpu
from jax.sharding import PartitionSpec as P

EPS = 0.05
BETA = 0.9
RATE_BASE = 0.5
MESH = pl.DeviceIdType.MESH
LANES = 128


class Gather:
    def __init__(self, n, slot, send, recv, hook=None):
        me = lax.axis_index("fs")
        self.slot, self.send, self.recv, self.hook = slot, send, recv, hook
        self.n, self.me, self.places = n, me, n // 2
        self.place, self.parity = me // 2, me % 2
        self.partner = me + 1 - 2 * self.parity
        self.started = []

    def put(self, cond, index, half, way):
        target = (self.me - 2, self.me + 2, self.partner)[way]
        if way == 0:
            cond = jnp.logical_and(cond, self.place > 0)
        elif way == 1:
            cond = jnp.logical_and(cond, self.place < self.places - 1)

        def make():
            return pltpu.make_async_remote_copy(
                src_ref=self.slot(index, half),
                dst_ref=self.slot(index, half),
                send_sem=self.send.at[index, half, way],
                recv_sem=self.recv.at[index, half],
                device_id={"fs": target},
                device_id_type=MESH,
            )

        @pl.when(cond)
        def _():
            make().start()

        self.started.append((cond, make))

    def arrive(self, cond, index, half):
        @pl.when(cond)
        def _():
            pltpu.make_async_remote_copy(
                src_ref=self.slot(index, half),
                dst_ref=self.slot(index, half),
                send_sem=self.send.at[index, half, 0],
                recv_sem=self.recv.at[index, half],
                device_id={"fs": self.partner},
                device_id_type=MESH,
            ).wait_recv()
            if self.hook is not None:
                self.hook(index, half)

    def begin(self):
        true = self.me >= 0
        for half in (0, 1):
            for way in (2, 0, 1):
                self.put(true, self.me, half, way)

    def turn(self):
        true = self.me >= 0
        self.arrive(true, self.partner, 0)
        for way in (0, 1):
            self.put(true, self.partner, 0, way)

    def step(self, s):
        for way in (1, 0):
            place = self.place - s if way == 1 else self.place + s
            cond = jnp.logical_and(place >= 0, place < self.places)
            same = 2 * place + self.parity
            other = 2 * place + 1 - self.parity
            self.arrive(cond, same, 1)
            self.put(cond, same, 1, 2)
            self.put(cond, same, 1, way)
            self.arrive(cond, same, 0)
            self.put(cond, same, 0, way)
            self.arrive(cond, other, 0)
            self.put(cond, other, 0, way)

    def finish_recv(self):
        true = self.me >= 0
        for place in range(self.places):
            self.arrive(true, 2 * place + 1 - self.parity, 1)

    def finish_send(self):
        for cond, make in self.started:

            @pl.when(cond)
            def _(make=make):
                make().wait_send()


def split(ref, t, tiles, count):
    return ref[pl.ds(t % tiles * 2 + t // tiles, count, stride=2 * tiles), :]


def head_step(head, q_ref, k_ref, v_ref, c_ref, mix_ref, gain_ref, dq_ref, dv_ref):
    length = q_ref.shape[0]
    width = gain_ref.shape[1]
    half = width // 2
    factor = half ** (-0.5)
    cols = slice(head * width, (head + 1) * width)
    query, key, value = q_ref[:, cols], k_ref[:, cols], v_ref[:, cols]
    lane = lax.broadcasted_iota(jnp.int32, (length, width), 1)
    zero = jnp.zeros_like(key)
    key0 = jnp.where(lane < half, key, zero)
    key1 = jnp.where(lane < half, zero, key)
    row = lax.broadcasted_iota(jnp.int32, (length, length), 0)
    col = lax.broadcasted_iota(jnp.int32, (length, length), 1)
    causal = col <= row
    mix = mix_ref[head]
    nt = (((1,), (1,)), ((), ()))
    tn = (((0,), (0,)), ((), ()))

    def probs(rows):
        scores = lax.dot_general(query, rows, nt, preferred_element_type=jnp.float32) * factor
        scores = jnp.where(causal, scores, -jnp.inf)
        expo = jnp.exp(scores - jnp.max(scores, axis=-1, keepdims=True))
        return expo * (1.0 / jnp.sum(expo, axis=-1, keepdims=True))

    first, second = probs(key0), probs(key1)
    mixed = (first - mix * second).astype(jnp.bfloat16)
    output = jnp.dot(mixed, value, preferred_element_type=jnp.float32)
    inverse = lax.rsqrt(jnp.mean(output * output, axis=-1, keepdims=True) + EPS)
    scaled = gain_ref[...] * c_ref[:, cols].astype(jnp.float32)
    d_out = inverse * scaled - output * (inverse * inverse * inverse) * jnp.mean(
        output * scaled, axis=-1, keepdims=True
    )
    d_out = d_out.astype(jnp.bfloat16)
    dv_ref[:, cols] = lax.dot_general(mixed, d_out, tn, preferred_element_type=jnp.float32).astype(jnp.bfloat16)
    d_mix = lax.dot_general(d_out, value, nt, preferred_element_type=jnp.float32)
    d_first = first * (d_mix - jnp.sum(first * d_mix, axis=-1, keepdims=True))
    d_second = -mix * second * (d_mix - jnp.sum(second * d_mix, axis=-1, keepdims=True))
    d_query = jnp.dot(d_first.astype(jnp.bfloat16), key0, preferred_element_type=jnp.float32)
    d_query += jnp.dot(d_second.astype(jnp.bfloat16), key1, preferred_element_type=jnp.float32)
    dq_ref[:, cols] = (d_query * factor).astype(jnp.bfloat16)


def kernel(
    n, tp, heads,
    x_ref, q_ref, k_ref, v_ref, c_ref, mix_ref, gain_ref, f_ref, mom_ref, w_ref,
    fall, wall, nmall, nm_ref, tot_ref, fown,
    fwide, dq, dv, psend, precv, sums,
    f_send, f_recv, s_send, s_recv, w_send, w_recv, n_send, n_recv, p_send, p_recv, t_send, t_recv,
):
    me = lax.axis_index("fs")
    mt = lax.axis_index("tp")
    deep = fown.shape[0]
    part = deep // 2
    cut = max(16, deep // 64 * 16)
    rank = fown.shape[1] // 2
    rank_here = rank // n
    cols = dq.shape[1]
    tiles_f, tiles_w = rank // LANES, cols // LANES
    here = pl.ds(pl.multiple_of(me * deep, deep), deep)
    fwide[...] = f_ref[...].astype(jnp.float32)
    for t in range(2 * tiles_f):
        block = split(fwide, t, tiles_f, deep).astype(jnp.bfloat16)
        fown[:, t * LANES : (t + 1) * LANES] = block
        fall[here, t * LANES : (t + 1) * LANES] = block
    barrier = pltpu.get_barrier_semaphore()
    for hop in range(1, n):
        pl.semaphore_signal(barrier, inc=1, device_id={"fs": (me + hop) % n}, device_id_type=MESH)
    for hop in range(1, tp):
        pl.semaphore_signal(barrier, inc=1, device_id={"tp": (mt + hop) % tp}, device_id_type=MESH)
    pl.semaphore_wait(barrier, n - 1 + tp - 1)

    def rows(ref):
        def slot(index, half):
            start, size = (cut, deep - cut) if half else (0, cut)
            return ref.at[pl.ds(pl.multiple_of(index * deep + start, 16), size)]

        return slot

    quarter = 2 * rank // tp
    far, near = (mt + 2) % tp, mt + 1 - 2 * (mt % 2)

    def quarters(index, half, which):
        return fall.at[
            pl.ds(pl.multiple_of(index * deep + half * part, part), part),
            pl.ds(pl.multiple_of(which * quarter, quarter), quarter),
        ]

    def spread(index, half, which, target, way):
        return pltpu.make_async_remote_copy(
            src_ref=quarters(index, half, which),
            dst_ref=quarters(index, half, which),
            send_sem=s_send.at[index, half, way],
            recv_sem=s_recv.at[index, half, way],
            device_id={"tp": target},
            device_id_type=MESH,
        )

    def hook(index, half):
        spread(index, half, mt, far, 0).start()
        spread(index, half, mt, near, 1).start()

    def spread_all():
        pieces = [((me + hop) % n, half) for hop in range(1, n) for half in (0, 1)]
        for index, half in pieces:
            spread(index, half, far, far, 0).wait_recv()
            spread(index, half, far, near, 2).start()
        for index, half in pieces:
            spread(index, half, near, near, 1).wait_recv()
            spread(index, half, (near + 2) % tp, near, 2).wait_recv()

    def spread_sent():
        for hop in range(1, n):
            for half in (0, 1):
                index = (me + hop) % n
                spread(index, half, mt, far, 0).wait_send()
                spread(index, half, mt, near, 1).wait_send()
                spread(index, half, far, near, 2).wait_send()

    if tp == 4 and quarter % LANES == 0:
        gather_f = Gather(n, lambda i, half: quarters(i, half, mt), f_send, f_recv, hook)
    else:
        spread_all = spread_sent = lambda: None
        gather_f = Gather(n, rows(fall), f_send, f_recv)
    gather_w = Gather(n, rows(wall), w_send, w_recv)
    gather_n = Gather(n, lambda i, half: nmall.at[i, half], n_send, n_recv)
    gather_f.begin()
    for t in range(2 * tiles_w):
        wall[here, t * LANES : (t + 1) * LANES] = split(w_ref, t, tiles_w, deep).astype(jnp.bfloat16)
    gather_w.begin()
    gather_f.turn()
    done = 1
    for head in range(heads):
        head_step(head, q_ref, k_ref, v_ref, c_ref, mix_ref, gain_ref, dq, dv)
        if done < n // 2:
            gather_f.step(done)
            done += 1
    for s in range(done, n // 2):
        gather_f.step(s)
    gather_w.turn()
    gather_f.finish_recv()
    spread_all()
    gather_w.step(1)
    for m, cot in enumerate((dq, dv)):
        reduced = jnp.dot(
            x_ref[...], fall[:, m * rank : (m + 1) * rank], preferred_element_type=jnp.float32
        ).astype(jnp.bfloat16)
        partial = lax.dot_general(
            reduced, cot[...], (((0,), (0,)), ((), ())), preferred_element_type=jnp.float32
        )
        for j in range(n):
            psend[j, m] = partial[j * rank_here : (j + 1) * rank_here].astype(psend.dtype)

    def p_copy(hop):
        peer = (me + hop) % n
        return pltpu.make_async_remote_copy(
            src_ref=psend.at[peer],
            dst_ref=precv.at[hop],
            send_sem=p_send.at[hop],
            recv_sem=p_recv.at[hop],
            device_id={"fs": peer},
            device_id_type=MESH,
        )

    for hop in range(1, n):
        p_copy(hop).start()
    for s in range(2, n // 2 - 1):
        gather_w.step(s)
    total = psend[me].astype(jnp.float32)
    for hop in range(1, n):
        p_copy(hop).wait_recv()
        total += precv[hop].astype(jnp.float32)
    length = x_ref.shape[0]
    for t in range(2 * tiles_w):
        m, lanes = t // tiles_w, slice(t % tiles_w * LANES, (t % tiles_w + 1) * LANES)
        moments = BETA * split(mom_ref, t, tiles_w, rank_here)
        moments += total[m, :, lanes] * (length * n) ** (-0.5)
        nm_ref[m, :, lanes] = moments
        nmall[me, m, :, lanes] = moments.astype(nmall.dtype)
    gather_n.begin()
    gather_w.step(n // 2 - 1)
    gather_n.turn()
    for s in range(1, n // 2):
        gather_n.step(s)
    gather_n.finish_recv()
    everything = nmall[...].astype(jnp.float32)
    squares = jnp.sum(jnp.sum(everything * everything, axis=0), axis=1)
    sums[0] = jnp.sum(squares, axis=1, keepdims=True) + jnp.zeros((2, 128), jnp.float32)

    def t_copy(hop):
        return pltpu.make_async_remote_copy(
            src_ref=sums.at[0],
            dst_ref=sums.at[hop],
            send_sem=t_send.at[hop],
            recv_sem=t_recv.at[hop],
            device_id={"tp": (mt + hop) % tp},
            device_id_type=MESH,
        )

    for hop in range(1, tp):
        t_copy(hop).start()
    gather_w.finish_recv()
    totals = sums[0]
    for hop in range(1, tp):
        t_copy(hop).wait_recv()
        totals += sums[hop]
    tot_ref[...] = totals
    for hop in range(1, tp):
        t_copy(hop).wait_send()
    for hop in range(1, n):
        p_copy(hop).wait_send()
    spread_sent()
    for gather in (gather_f, gather_w, gather_n):
        gather.finish_send()


def finish(entries, fall, wall, nmall, nm_ref, tot_ref, fown, step, nm_out, copies, wide):
    _, _, rank_here, cols = nmall.shape
    rank = fall.shape[1] // 2
    tiles = cols // LANES
    rate = RATE_BASE / jnp.sqrt(1.0 + tot_ref[...] / entries)

    def lows(rows, m):
        block = nmall[:, m].reshape(rank, cols).astype(jnp.bfloat16)
        return jnp.dot(
            rows[:, m * rank : (m + 1) * rank], block, preferred_element_type=jnp.float32
        )

    count = fall.shape[0]
    for m in range(2):
        low = lows(fall, m)
        for t in range(tiles):
            lanes = slice(t * LANES, (t + 1) * LANES)
            old = wall[:, m * cols + t * LANES : m * cols + (t + 1) * LANES].astype(jnp.float32)
            wide[pl.ds(2 * t + m, count, stride=2 * tiles), :] = (
                old - low[:, lanes] * rate[m : m + 1]
            )
    copies[...] = wide[...].astype(jnp.bfloat16)

    @pl.when(pl.program_id(0) == 0)
    def _():
        for m in range(2):
            low = lows(fown, m)
            for t in range(tiles):
                lanes = slice(t * LANES, (t + 1) * LANES)
                step[pl.ds(2 * t + m, fown.shape[0], stride=2 * tiles), :] = (
                    low[:, lanes] * rate[m : m + 1]
                )
                nm_out[pl.ds(2 * t + m, rank_here, stride=2 * tiles), :] = nm_ref[m, :, lanes]


def to_rows(array):
    rows, maps, cols = array.shape
    return array.reshape(rows, maps, cols // LANES, LANES).transpose(0, 2, 1, 3).reshape(-1, LANES)


def from_rows(array, rows):
    return (
        array.reshape(rows, -1, 2, LANES).transpose(0, 2, 1, 3).reshape(rows, 2, -1)
    )


def per_device(
    n, tp, inputs, queries, keys, values, head_cot, mixing, head_gain, factors, moments, weights
):
    length, depth = inputs.shape
    heads = mixing.shape[0]
    deep, _, rank = factors.shape
    rank_here, _, cols = moments.shape
    wire = jnp.bfloat16 if rank_here % 16 == 0 else jnp.float32
    vmem = pl.BlockSpec(memory_space=pltpu.VMEM)
    dma = pltpu.SemaphoreType.DMA
    held = pl.pallas_call(
        functools.partial(kernel, n, tp, heads),
        out_shape=(
            jax.ShapeDtypeStruct((depth, 2 * rank), jnp.bfloat16),
            jax.ShapeDtypeStruct((depth, 2 * cols), jnp.bfloat16),
            jax.ShapeDtypeStruct((n, 2, rank_here, cols), wire),
            jax.ShapeDtypeStruct((2, rank_here, cols), jnp.float32),
            jax.ShapeDtypeStruct((2, LANES), jnp.float32),
            jax.ShapeDtypeStruct((deep, 2 * rank), jnp.bfloat16),
        ),
        in_specs=[vmem] * 5 + [pl.BlockSpec(memory_space=pltpu.SMEM)] + [vmem] * 4,
        out_specs=(vmem,) * 6,
        scratch_shapes=[
            pltpu.VMEM((deep * 2 * rank // LANES, LANES), jnp.float32),
            pltpu.VMEM((length, cols), jnp.bfloat16),
            pltpu.VMEM((length, cols), jnp.bfloat16),
            pltpu.VMEM((n, 2, rank_here, cols), wire),
            pltpu.VMEM((n, 2, rank_here, cols), wire),
            pltpu.VMEM((tp, 2, LANES), jnp.float32),
            dma((n, 2, 3)), dma((n, 2)), dma((n, 2, 3)), dma((n, 2, 3)),
            dma((n, 2, 3)), dma((n, 2)),
            dma((n, 2, 3)), dma((n, 2)),
            dma((n,)), dma((n,)),
            dma((tp,)), dma((tp,)),
        ],
        compiler_params=pltpu.CompilerParams(
            collective_id=0, has_side_effects=True, vmem_limit_bytes=56 * 1024 * 1024
        ),
    )(
        inputs, queries, keys, values, head_cot, mixing, head_gain[None, :],
        to_rows(factors), to_rows(moments), to_rows(weights),
    )
    block = min(depth, 256)
    per_row = 2 * cols // LANES

    def whole(shape):
        return pl.BlockSpec(shape, lambda i: (0,) * len(shape))

    step, new_moments, copies = pl.pallas_call(
        functools.partial(finish, rank * cols * tp),
        grid=(depth // block,),
        out_shape=(
            jax.ShapeDtypeStruct((deep * per_row, LANES), jnp.float32),
            jax.ShapeDtypeStruct((rank_here * per_row, LANES), jnp.float32),
            jax.ShapeDtypeStruct((depth * per_row, LANES), jnp.bfloat16),
        ),
        in_specs=[
            pl.BlockSpec((block, 2 * rank), lambda i: (i, 0)),
            pl.BlockSpec((block, 2 * cols), lambda i: (i, 0)),
            whole((n, 2, rank_here, cols)),
            whole((2, rank_here, cols)),
            whole((2, LANES)),
            whole((deep, 2 * rank)),
        ],
        out_specs=(
            whole((deep * per_row, LANES)),
            whole((rank_here * per_row, LANES)),
            pl.BlockSpec((block * per_row, LANES), lambda i: (i, 0)),
        ),
        scratch_shapes=[pltpu.VMEM((block * per_row, LANES), jnp.float32)],
    )(*held)
    return from_rows(step, deep), from_rows(new_moments, rank_here), from_rows(copies, depth)


def solution(mesh):
    placed = (
        P("fs", None),
        P("fs", "tp"),
        P("fs", "tp"),
        P("fs", "tp"),
        P("fs", "tp"),
        P("tp"),
        P(),
        P("fs", None, None),
        P("fs", None, "tp"),
        P("fs", None, "tp"),
    )
    return jax.shard_map(
        functools.partial(per_device, mesh.shape["fs"], mesh.shape["tp"]),
        mesh=mesh,
        in_specs=placed,
        out_specs=(P("fs", None, "tp"), P("fs", None, "tp"), P(None, None, "tp")),
        check_vma=False,
    )
```

profile of v0, /device:TPU:0, one launch (start us, length us, event | category | flops | bytes accessed | tf_op | source)
XLA Modules:
  0.0 102.9 jit_solution(9811179509677707119)
XLA Ops:
  0.6 93.0 %shard_map.121 = (bf16[2048,512]{1,0:T(8,128)(2,1)}, bf16[2048,1024]{1,0:T(8,128)(2,1)}, bf16[8,2,32,512]{3,2,1,0:T(8,128)(2,1)}, f32[2,32,512]{2,1,0:T(8,128)},...) custom-call(bf16[384,2048]{1,0:T(8,128)(2,1)} %x_ref.1, bf16[384,512]{1,0:T(8,128)(2,1)} %q_ref.1, bf16[384,512]{1,0:T(8,128)(2,1)} %k_ref.1, ...), custom_call_target="tpu_custom_call" | custom-call | tf_op jit(solution)/shard_map/pallas_call | solution.py:377
  93.6 9.3 %shard_map.122 = (f32[2048,128]{1,0:T(8,128)}, f32[256,128]{1,0:T(8,128)}, bf16[16384,128]{1,0:T(8,128)(2,1)}) custom-call(bf16[2048,512]{1,0:T(8,128)(2,1)} %get-tuple-element.12.fall, bf16[2048,1024]{1,0:T(8,128)(2,1)} %get-tuple-element.13.wall, bf16[8,2,32,512]{3,2,1,0:T(8,128)(2,1)} %get-tuple-element.14.nmall, f32[2,32,512]{2,1,0:T(8,128)} %get-tuple-element.15.nm_ref, ...), custom_call_target="tpu_custom_call" | custom-call | tf_op jit(solution)/shard_map/pallas_call | solution.py:415
where the time goes:
time: 103 us
  Pallas kernels  102 us (99%)
    pallas_call x1, Pallas kernels, per_device(): pl.pallas_call(functools.partial(kernel, n, tp, heads), out_shape=(jax.Sh...  93 us
    pallas_call x1, Pallas kernels, per_device(): pl.pallas_call(functools.partial(finish, rank * cols * tp), grid=(depth /...  9.28 us

commit v1 on v0

v1 whole, which is shorter than its diff:
```python
import functools

import jax
import jax.numpy as jnp
from jax import lax
from jax.experimental import pallas as pl
from jax.experimental.pallas import tpu as pltpu
from jax.sharding import PartitionSpec as P

EPS = 0.05
BETA = 0.9
RATE_BASE = 0.5
MESH = pl.DeviceIdType.MESH
LANES = 128
CHUNKS = 8
WIDE = 1
DEPTH = 2


def split(ref, t, tiles, count):
    return ref[pl.ds(t % tiles * 2 + t // tiles, count, stride=2 * tiles), :]


def head_step(head, q_ref, k_ref, v_ref, c_ref, mix_ref, gain_ref, dq_ref, dv_ref):
    length = q_ref.shape[0]
    width = gain_ref.shape[1]
    half = width // 2
    factor = half ** (-0.5)
    cols = slice(head * width, (head + 1) * width)
    query, key, value = q_ref[:, cols], k_ref[:, cols], v_ref[:, cols]
    lane = lax.broadcasted_iota(jnp.int32, (length, width), 1)
    zero = jnp.zeros_like(key)
    key0 = jnp.where(lane < half, key, zero)
    key1 = jnp.where(lane < half, zero, key)
    row = lax.broadcasted_iota(jnp.int32, (length, length), 0)
    col = lax.broadcasted_iota(jnp.int32, (length, length), 1)
    causal = col <= row
    mix = mix_ref[head]
    nt = (((1,), (1,)), ((), ()))
    tn = (((0,), (0,)), ((), ()))

    def probs(rows):
        scores = lax.dot_general(query, rows, nt, preferred_element_type=jnp.float32) * factor
        scores = jnp.where(causal, scores, -jnp.inf)
        expo = jnp.exp(scores - jnp.max(scores, axis=-1, keepdims=True))
        return expo * (1.0 / jnp.sum(expo, axis=-1, keepdims=True))

    first, second = probs(key0), probs(key1)
    mixed = (first - mix * second).astype(jnp.bfloat16)
    output = jnp.dot(mixed, value, preferred_element_type=jnp.float32)
    inverse = lax.rsqrt(jnp.mean(output * output, axis=-1, keepdims=True) + EPS)
    scaled = gain_ref[...] * c_ref[:, cols].astype(jnp.float32)
    d_out = inverse * scaled - output * (inverse * inverse * inverse) * jnp.mean(
        output * scaled, axis=-1, keepdims=True
    )
    d_out = d_out.astype(jnp.bfloat16)
    dv_ref[:, cols] = lax.dot_general(mixed, d_out, tn, preferred_element_type=jnp.float32).astype(jnp.bfloat16)
    d_mix = lax.dot_general(d_out, value, nt, preferred_element_type=jnp.float32)
    d_first = first * (d_mix - jnp.sum(first * d_mix, axis=-1, keepdims=True))
    d_second = -mix * second * (d_mix - jnp.sum(second * d_mix, axis=-1, keepdims=True))
    d_query = jnp.dot(d_first.astype(jnp.bfloat16), key0, preferred_element_type=jnp.float32)
    d_query += jnp.dot(d_second.astype(jnp.bfloat16), key1, preferred_element_type=jnp.float32)
    dq_ref[:, cols] = (d_query * factor).astype(jnp.bfloat16)


class Lists:
    def __init__(self):
        def source(k, order):
            return [(k, True, c) for c in order] + [(k, False, c) for c in range(WIDE)]

        order = list(range(WIDE, CHUNKS)) + list(range(WIDE))
        mirror = lambda entries: [(3 - k, same, c) for k, same, c in entries]
        first = source(0, order)
        inner = source(1, order)
        self.up = {0: first, 1: self.merge(inner, first)}
        far = mirror(self.up[1])
        self.down = {0: [], 1: self.merge(inner, far)}
        self.from_up = {0: self.down[1], 1: far}
        self.from_down = {0: [], 1: first}
        own = lambda q: [(q, True, c) for c in range(CHUNKS)]
        narrow = lambda entries: [e for e in entries if e[1] and e[2] >= WIDE]
        self.cross = {
            0: own(0) + narrow(self.from_up[0]),
            1: own(1) + self.weave(narrow(self.from_down[1]), narrow(self.from_up[1])),
        }
        self.from_cross = {q: [(k, not same, c) for k, same, c in self.cross[q]] for q in (0, 1)}

    @staticmethod
    def merge(own, passed):
        return own + passed

    @staticmethod
    def weave(a, b):
        out = []
        for i in range(max(len(a), len(b))):
            out += a[i : i + 1] + b[i : i + 1]
        return out


class Weights:
    def __init__(self, lists, q):
        self.q = q
        self.out = {"up": list(lists.up[q]), "down": list(lists.down[q]), "cross": list(lists.cross[q])}
        self.into = {
            "cross": list(lists.from_cross[q]), "down": list(lists.from_down[q]), "up": list(lists.from_up[q]),
        }
        self.have = {(q, True, c) for c in range(CHUNKS)}
        self.got = {way: 0 for way in self.into}
        self.put = {way: 0 for way in self.out}
        self.round = 0

    def fill(self, depth, limit=None):
        moves = []
        for way in ("up", "down", "cross"):
            while self.put[way] < min(len(self.out[way]), self.round + depth):
                entry = self.out[way][self.put[way]]
                if entry not in self.have:
                    break
                moves.append(("send", way, entry))
                self.put[way] += 1
        return moves

    def turn(self, lag, depth):
        moves = self.fill(depth)
        self.round += 1
        for way in ("cross", "down", "up"):
            while self.got[way] < min(len(self.into[way]), self.round - lag):
                entry = self.into[way][self.got[way]]
                moves.append(("wait", way, entry))
                self.have.add(entry)
                self.got[way] += 1
                moves += self.fill(depth)
        return moves

    def done(self):
        return all(self.got[w] == len(self.into[w]) for w in self.into) and all(
            self.put[w] == len(self.out[w]) for w in self.out
        )


def kernel(
    n, tp, heads,
    x_hbm, q_hbm, k_hbm, v_hbm, c_hbm, mix_hbm, gain_hbm, f_hbm, mom_hbm, w_hbm,
    wall, low, nm_ref, tot_ref,
    x_ref, q_ref, k_ref, v_ref, c_ref, mix_ref, gain_ref, f_ref, mom_ref, w_ref,
    fall, nmall, fwide, dq, dv, psend, precv, sums,
    l_sem, f_send, f_recv, s_send, s_recv, w_send, w_recv, n_send, n_recv, p_send, p_recv, t_send, t_recv,
):
    me = lax.axis_index("fs")
    mt = lax.axis_index("tp")
    depth = fall.shape[0]
    deep = depth // n
    rank = fall.shape[1] // 2
    rank_here = rank // n
    cols = dq.shape[1]
    tiles_f, tiles_w = rank // LANES, cols // LANES
    per_row = 2 * tiles_w

    local = {}
    for i, (name, src, dst) in enumerate((
        ("f", f_hbm, f_ref), ("w", w_hbm, w_ref), ("gain", gain_hbm, gain_ref), ("mix", mix_hbm, mix_ref),
        ("q", q_hbm, q_ref), ("k", k_hbm, k_ref), ("v", v_hbm, v_ref), ("c", c_hbm, c_ref),
        ("x", x_hbm, x_ref), ("mom", mom_hbm, mom_ref),
    )):
        local[name] = pltpu.make_async_copy(src, dst, l_sem.at[i])
        local[name].start()

    barrier = pltpu.get_barrier_semaphore()
    for hop in range(1, n):
        pl.semaphore_signal(barrier, inc=1, device_id={"fs": (me + hop) % n}, device_id_type=MESH)
    for hop in range(1, tp):
        pl.semaphore_signal(barrier, inc=1, device_id={"tp": (mt + hop) % tp}, device_id_type=MESH)

    local["f"].wait()
    fwide[...] = f_ref[...].astype(jnp.float32)
    here = pl.ds(pl.multiple_of(me * deep, deep), deep)
    for t in range(2 * tiles_f):
        fall[here, t * LANES : (t + 1) * LANES] = split(fwide, t, tiles_f, deep).astype(jnp.bfloat16)
    local["w"].wait()
    wall[pl.ds(pl.multiple_of(me * deep * per_row, 16), deep * per_row), :] = w_ref[...].astype(jnp.bfloat16)
    for name in ("gain", "mix", "q", "k", "v", "c"):
        local[name].wait()

    def head(i):
        head_step(i, q_ref, k_ref, v_ref, c_ref, mix_ref, gain_ref, dq, dv)

    def remote(src, send, recv, axis, target):
        return pltpu.make_async_remote_copy(
            src_ref=src, dst_ref=src, send_sem=send, recv_sem=recv, device_id={axis: target}, device_id_type=MESH
        )

    def project():
        local["x"].wait()
        for m, cot in enumerate((dq, dv)):
            reduced = jnp.dot(
                x_ref[...], fall[:, m * rank : (m + 1) * rank], preferred_element_type=jnp.float32
            ).astype(jnp.bfloat16)
            partial = lax.dot_general(
                reduced, cot[...], (((0,), (0,)), ((), ())), preferred_element_type=jnp.float32
            )
            for j in range(n):
                psend[j, m] = partial[j * rank_here : (j + 1) * rank_here].astype(psend.dtype)

    def p_copy(hop):
        peer = (me + hop) % n
        return pltpu.make_async_remote_copy(
            src_ref=psend.at[peer], dst_ref=precv.at[hop], send_sem=p_send.at[hop], recv_sem=p_recv.at[hop],
            device_id={"fs": peer}, device_id_type=MESH,
        )

    def momentum():
        local["mom"].wait()
        total = psend[me].astype(jnp.float32)
        for hop in range(1, n):
            p_copy(hop).wait_recv()
            total += precv[hop].astype(jnp.float32)
        length = x_ref.shape[0]
        for t in range(2 * tiles_w):
            m, lanes = t // tiles_w, slice(t % tiles_w * LANES, (t % tiles_w + 1) * LANES)
            moments = BETA * split(mom_ref, t, tiles_w, rank_here)
            moments += total[m, :, lanes] * (length * n) ** (-0.5)
            nm_ref[pl.ds(t % tiles_w * 2 + m, rank_here, stride=per_row), :] = moments
            nmall[me, m, :, lanes] = moments.astype(nmall.dtype)

    def t_copy(hop):
        return pltpu.make_async_remote_copy(
            src_ref=sums.at[0], dst_ref=sums.at[hop], send_sem=t_send.at[hop], recv_sem=t_recv.at[hop],
            device_id={"tp": (mt + hop) % tp}, device_id_type=MESH,
        )

    def squares():
        everything = nmall[...].astype(jnp.float32)
        parts = jnp.sum(jnp.sum(everything * everything, axis=0), axis=1)
        sums[0] = jnp.sum(parts, axis=1, keepdims=True) + jnp.zeros((2, LANES), jnp.float32)
        for hop in range(1, tp):
            t_copy(hop).start()

    def totals():
        result = sums[0]
        for hop in range(1, tp):
            t_copy(hop).wait_recv()
            result += sums[hop]
        tot_ref[...] = result

    def lows(start, count):
        for m in range(2):
            block = nmall[:, m].reshape(rank, cols).astype(jnp.bfloat16)
            product = jnp.dot(
                fall[start : start + count, m * rank : (m + 1) * rank], block, preferred_element_type=jnp.float32
            )
            for t in range(tiles_w):
                low[pl.ds(start * per_row + 2 * t + m, count, stride=per_row), :] = (
                    product[:, t * LANES : (t + 1) * LANES]
                )

    def weights(index, chunk, chunks):
        size = deep // chunks * per_row
        return wall.at[pl.ds(pl.multiple_of(index * deep * per_row + chunk * size, 16), size)]

    quarter = 2 * rank // tp
    if n == 8 and tp == 4 and quarter % LANES == 0 and deep % (2 * CHUNKS) == 0:
        place, parity = me // 2, me % 2
        flip = place // 2
        side = jnp.where(flip == 0, place, 3 - place)
        lists = Lists()
        states = [Weights(lists, q) for q in (0, 1)]
        partner = me + 1 - 2 * parity
        far, near = (mt + 2) % tp, mt + 1 - 2 * (mt % 2)

        def index_of(k, same):
            return 2 * (k + flip * (3 - 2 * k)) + (parity if same else 1 - parity)

        def target(q, way):
            return partner if way == "cross" else index_of(q + 1 if way == "up" else q - 1, True)

        ways = {"up": 0, "down": 1, "cross": 2}

        def w_copy(q, way, entry):
            k, same, chunk = entry
            index = index_of(k, same)
            return remote(
                weights(index, chunk, CHUNKS), w_send.at[index, chunk, ways[way]], w_recv.at[index, chunk],
                "fs", target(q, way),
            )

        def run(q, moves):
            for kind, way, entry in moves:
                if kind == "send":
                    w_copy(q, way, entry).start()
                else:
                    w_copy(q, "cross", entry).wait_recv()

        def piece(index, which):
            return fall.at[
                pl.ds(pl.multiple_of(index * deep, deep), deep), pl.ds(pl.multiple_of(which * quarter, quarter), quarter)
            ]

        def others(q):
            return sorted((k for k in range(4) if k != q), key=lambda k: (abs(k - q), k))

        def small(kind, index, way, to):
            if kind == "f":
                return remote(piece(index, mt), f_send.at[index, way], f_recv.at[index], "fs", to)
            return remote(nmall.at[index], n_send.at[index, way], n_recv.at[index], "fs", to)

        def small_begin(kind, q):
            for i, k in enumerate(reversed(others(q))):
                small(kind, me, i, index_of(k, True)).start()
            small(kind, me, 3, partner).start()

        def spread(index, which, to, way):
            return remote(piece(index, which), s_send.at[index, way], s_recv.at[index, way], "tp", to)

        def small_wait(kind, q, k, same):
            index = index_of(k, same)
            small(kind, index, 0, partner).wait_recv()
            if same:
                small(kind, index, 0, partner).start()
            if kind == "f":
                spread(index, mt, far, 0).start()
                spread(index, mt, near, 1).start()

        def pieces(q):
            return [(q, False)] + [(k, True) for k in others(q)] + [(k, False) for k in others(q)]

        def segment(tokens):
            for q in (0, 1):

                @pl.when(side == q)
                def _(q=q):
                    for token in tokens:
                        kind, *rest = token
                        if kind == "w":
                            lag, count = rest
                            for _ in range(count):
                                run(q, states[q].turn(lag, DEPTH))
                        elif kind == "begin":
                            small_begin(rest[0], q)
                        elif kind == "fill":
                            run(q, states[q].fill(rest[0]))
                        elif kind == "small":
                            for i in rest[1]:
                                small_wait(rest[0], q, *pieces(q)[i])
                        elif kind == "all":
                            while not states[q].done():
                                run(q, states[q].turn(*rest, DEPTH))
                        elif kind == "spread":
                            for k, same in pieces(q):
                                index = index_of(k, same)
                                spread(index, far, far, 0).wait_recv()
                                spread(index, far, near, 2).start()
                            for k, same in pieces(q):
                                index = index_of(k, same)
                                spread(index, near, near, 1).wait_recv()
                                spread(index, (near + 2) % tp, near, 2).wait_recv()
                        elif kind == "sent":
                            for way in ways:
                                for entry in states[q].out[way]:
                                    w_copy(q, way, entry).wait_send()
                            for name in ("f", "n"):
                                for way in range(4):
                                    small(name, me, way, partner).wait_send()
                                for k in others(q):
                                    small(name, index_of(k, True), 0, partner).wait_send()
                            for k, same in pieces(q):
                                for way in range(3):
                                    spread(index_of(k, same), mt, near, way).wait_send()

        head(0)
        pl.semaphore_wait(barrier, n - 1 + tp - 1)
        segment([("begin", "f"), ("fill", DEPTH)])
        head(1)
        segment([("small", "f", (0,)), ("w", 4, 1)])
        head(2)
        segment([("small", "f", (1, 2)), ("w", 4, 1)])
        head(3)
        for i in range(4, heads):
            head(i)
        segment([("w", 4, 1), ("small", "f", (3,)), ("w", 4, 2), ("small", "f", (4, 5, 6)), ("w", 4, 1), ("spread",)])
        project()
        for hop in range(1, n):
            p_copy(hop).start()
        segment([("w", 4, 8)])
        momentum()
        segment([
            ("begin", "n"), ("w", 4, 2), ("small", "n", (0, 1, 2)), ("w", 4, 2), ("small", "n", (3,)), ("w", 4, 2),
            ("small", "n", (4, 5, 6)),
        ])
        squares()
        for j in range(n):
            lows(j * deep, deep)
            segment([("w", 4, 1)])
        totals()
        segment([("all", 4)])
        segment([("sent",)])
    else:
        for i in range(heads):
            head(i)
        pl.semaphore_wait(barrier, n - 1 + tp - 1)

        def block(kind, index, hop):
            if kind == "f":
                return remote(
                    fall.at[pl.ds(pl.multiple_of(index * deep, 8), deep)], f_send.at[hop], f_recv.at[index],
                    "fs", (me + hop) % n,
                )
            if kind == "w":
                return remote(weights(index, 0, 1), w_send.at[hop], w_recv.at[index], "fs", (me + hop) % n)
            return remote(nmall.at[index], n_send.at[hop], n_recv.at[index], "fs", (me + hop) % n)

        def each(action):
            def step(hop, carry):
                action(hop)
                return carry

            lax.fori_loop(1, n, step, 0)

        each(lambda hop: block("f", me, hop).start())
        each(lambda hop: block("w", me, hop).start())
        each(lambda hop: block("f", (me + hop) % n, hop).wait_recv())
        project()
        each(lambda hop: p_copy(hop).start())
        momentum()
        each(lambda hop: block("n", me, hop).start())
        each(lambda hop: block("n", (me + hop) % n, hop).wait_recv())
        squares()
        for start in range(0, depth, 256):
            lows(start, min(256, depth - start))
        totals()
        each(lambda hop: block("w", (me + hop) % n, hop).wait_recv())
        for kind in ("f", "w", "n"):
            each(lambda hop, kind=kind: block(kind, me, hop).wait_send())
    for hop in range(1, tp):
        t_copy(hop).wait_send()
    for hop in range(1, n):
        p_copy(hop).wait_send()


def finish(n, entries, wall, low, nm_ref, tot_ref, step_hbm, nm_hbm, copies_hbm, step, copies, sems):
    me = lax.axis_index("fs")
    rows = low.shape[0]
    own = rows // n
    nm_copy = pltpu.make_async_copy(nm_ref, nm_hbm, sems.at[0])
    nm_copy.start()
    rate = RATE_BASE / jnp.sqrt(1.0 + tot_ref[...] / entries)
    count = min(rows // 16, 1024)
    odd = lax.broadcasted_iota(jnp.int32, (count, LANES), 0) % 2 == 1
    rates = jnp.where(odd, rate[1:2], rate[0:1])
    started = [nm_copy]
    for i in range(0, own, min(count, own)):
        size = min(count, own)
        start = pl.multiple_of(me * own + i, 8)
        step[i : i + size, :] = low[pl.ds(start, size), :] * rates[:size]
    started.append(pltpu.make_async_copy(step, step_hbm, sems.at[1]))
    started[-1].start()
    for i in range(rows // count):
        at = slice(i * count, (i + 1) * count)
        copies[at, :] = (wall[at, :].astype(jnp.float32) - low[at, :] * rates).astype(jnp.bfloat16)
        started.append(pltpu.make_async_copy(copies.at[at], copies_hbm.at[at], sems.at[2 + i]))
        started[-1].start()
    for copy in started:
        copy.wait()


def to_rows(array):
    rows, maps, cols = array.shape
    return array.reshape(rows, maps, cols // LANES, LANES).transpose(0, 2, 1, 3).reshape(-1, LANES)


def from_rows(array, rows):
    return (
        array.reshape(rows, -1, 2, LANES).transpose(0, 2, 1, 3).reshape(rows, 2, -1)
    )


def per_device(
    n, tp, inputs, queries, keys, values, head_cot, mixing, head_gain, factors, moments, weights
):
    length, depth = inputs.shape
    heads = mixing.shape[0]
    deep, _, rank = factors.shape
    rank_here, _, cols = moments.shape
    wire = jnp.bfloat16 if rank_here % 16 == 0 else jnp.float32
    per_row = 2 * cols // LANES
    hbm = pl.BlockSpec(memory_space=pltpu.HBM)
    vmem = pl.BlockSpec(memory_space=pltpu.VMEM)
    dma = pltpu.SemaphoreType.DMA
    args = (
        inputs, queries, keys, values, head_cot, mixing, head_gain[None, :],
        to_rows(factors), to_rows(moments), to_rows(weights),
    )
    held = pl.pallas_call(
        functools.partial(kernel, n, tp, heads),
        out_shape=(
            pltpu.VMEM((depth * per_row, LANES), jnp.bfloat16),
            pltpu.VMEM((depth * per_row, LANES), jnp.float32),
            pltpu.VMEM((rank_here * per_row, LANES), jnp.float32),
            pltpu.VMEM((2, LANES), jnp.float32),
        ),
        in_specs=[hbm] * len(args),
        out_specs=(vmem,) * 4,
        scratch_shapes=[
            pltpu.VMEM((length, depth), jnp.bfloat16),
            pltpu.VMEM((length, cols), jnp.bfloat16),
            pltpu.VMEM((length, cols), jnp.bfloat16),
            pltpu.VMEM((length, cols), jnp.bfloat16),
            pltpu.VMEM((length, cols), jnp.bfloat16),
            pltpu.SMEM((heads,), jnp.float32),
            pltpu.VMEM((1, head_gain.shape[0]), jnp.float32),
            pltpu.VMEM((deep * 2 * rank // LANES, LANES), jnp.bfloat16),
            pltpu.VMEM((rank_here * per_row, LANES), jnp.float32),
            pltpu.VMEM((deep * per_row, LANES), jnp.float32),
            pltpu.VMEM((depth, 2 * rank), jnp.bfloat16),
            pltpu.VMEM((n, 2, rank_here, cols), wire),
            pltpu.VMEM((deep * 2 * rank // LANES, LANES), jnp.float32),
            pltpu.VMEM((length, cols), jnp.bfloat16),
            pltpu.VMEM((length, cols), jnp.bfloat16),
            pltpu.VMEM((n, 2, rank_here, cols), wire),
            pltpu.VMEM((n, 2, rank_here, cols), wire),
            pltpu.VMEM((tp, 2, LANES), jnp.float32),
            dma((len(args),)),
            *(
                (
                    dma((n, 4)), dma((n,)), dma((n, 3)), dma((n, 3)),
                    dma((n, CHUNKS, 3)), dma((n, CHUNKS)), dma((n, 4)), dma((n,)),
                )
                if n == 8
                else (dma((n,)), dma((n,)), dma((1,)), dma((1,)), dma((n,)), dma((n,)), dma((n,)), dma((n,)))
            ),
            dma((n,)), dma((n,)),
            dma((tp,)), dma((tp,)),
        ],
        compiler_params=pltpu.CompilerParams(
            collective_id=0, has_side_effects=True, vmem_limit_bytes=36 * 1024 * 1024
        ),
    )(*(pltpu.with_memory_space_constraint(arg, pltpu.HBM) for arg in args))
    out_hbm = pl.BlockSpec(memory_space=pltpu.HBM)
    step, new_moments, copies = pl.pallas_call(
        functools.partial(finish, n, rank * cols * tp),
        out_shape=(
            jax.ShapeDtypeStruct((deep * per_row, LANES), jnp.float32),
            jax.ShapeDtypeStruct((rank_here * per_row, LANES), jnp.float32),
            jax.ShapeDtypeStruct((depth * per_row, LANES), jnp.bfloat16),
        ),
        in_specs=[vmem] * 4,
        out_specs=(out_hbm,) * 3,
        scratch_shapes=[
            pltpu.VMEM((deep * per_row, LANES), jnp.float32),
            pltpu.VMEM((depth * per_row, LANES), jnp.bfloat16),
            dma((18,)),
        ],
        compiler_params=pltpu.CompilerParams(vmem_limit_bytes=16 * 1024 * 1024),
    )(*held)
    return from_rows(step, deep), from_rows(new_moments, rank_here), from_rows(copies, depth)


def solution(mesh):
    placed = (
        P("fs", None),
        P("fs", "tp"),
        P("fs", "tp"),
        P("fs", "tp"),
        P("fs", "tp"),
        P("tp"),
        P(),
        P("fs", None, None),
        P("fs", None, "tp"),
        P("fs", None, "tp"),
    )
    return jax.shard_map(
        functools.partial(per_device, mesh.shape["fs"], mesh.shape["tp"]),
        mesh=mesh,
        in_specs=placed,
        out_specs=(P("fs", None, "tp"), P("fs", None, "tp"), P(None, None, "tp")),
        check_vma=False,
    )
```

time: 103 us -> 85.8 us (0.83)
  Pallas kernels: 102 us -> 85.1 us
    pallas_call x2, Pallas kernels: 102 us -> 85.1 us  [the longest x1 82.4 us: per_device(): pl.pallas_call(functools.partial(kernel, n, tp, heads), out_shape=(pltpu....]
where the time goes in v1:
time: 85.8 us; the launch traced here: 85.7 us
  Pallas kernels  85.1 us (99%)
    pallas_call x1, Pallas kernels, per_device(): pl.pallas_call(functools.partial(kernel, n, tp, heads), out_shape=(pltpu....  82.4 us
    pallas_call x1, Pallas kernels, per_device(): pl.pallas_call(functools.partial(finish, n, rank * cols * tp), out_shape=...  2.62 us

profile of v1, /device:TPU:0, one launch (start us, length us, event | category | flops | bytes accessed | tf_op | source)
XLA Modules:
  0.0 85.7 jit_solution(17793513561528290755)
XLA Ops:
  0.6 82.4 %shard_map.121 = (bf16[16384,128]{1,0:T(8,128)(2,1)S(1)}, f32[16384,128]{1,0:T(8,128)S(1)}, f32[256,128]{1,0:T(8,128)S(1)}, f32[2,128]{1,0:T(2,128)S(1)}) custom-call(bf16[384,2048]{1,0:T(8,128)(2,1)} %x_hbm.1, bf16[384,512]{1,0:T(8,128)(2,1)} %q_hbm.1, bf16[384,512]{1,0:T(8,128)(2,1)} %k_hbm.1, bf16[384,512]{1,0:T(8,128)(2,1)} %v_hbm.1, ...), custom_call_target="tpu_custom_call" | custom-call | tf_op jit(solution)/shard_map/pallas_call | solution.py:492
  83.1 2.6 %shard_map.122 = (f32[2048,128]{1,0:T(8,128)}, f32[256,128]{1,0:T(8,128)}, bf16[16384,128]{1,0:T(8,128)(2,1)}) custom-call(bf16[16384,128]{1,0:T(8,128)(2,1)S(1)} %get-tuple-element.10.wall, f32[16384,128]{1,0:T(8,128)S(1)} %get-tuple-element.11.low, f32[256,128]{1,0:T(8,128)S(1)} %get-tuple-element.12.nm_ref, f32[2,128]{1,0:T(2,128)S(1)} %get-tuple-element.13.tot_ref), custom_call_target="tpu_custom_call" | custom-call | tf_op jit(solution)/shard_map/pallas_call | solution.py:538

commit v2 on v1

--- a/solution.py
+++ b/solution.py
@@ -13,8 +13,32 @@
 MESH = pl.DeviceIdType.MESH
 LANES = 128
 CHUNKS = 8
-WIDE = 1
-DEPTH = 2
+WIDE = 2
+DIRECT = ()
+SCHEDULE = [
+    ("begin", "f"), ("w", 0, 0, 4, 2),
+    ("head", 1),
+    ("small", "f", (0,)), ("w", 0, 0, 5, 2),
+    ("head", 2),
+    ("small", "f", (1, 2)), ("w", 0, 0, 10, 2),
+    ("head", 3),
+    ("small", "f", (3,)), ("w", 0, 0, 10, 8), ("small", "f", (4, 5, 6)), ("spread",),
+    ("w", 6, 6, 12, 10),
+    ("project",),
+    ("px",), ("w", 8, 8, 14, 10), ("w", 9, 8, 15, 10),
+    ("pz", (0,)), ("w", 10, 8, 15, 10), ("pz", (1,)), ("w", 11, 8, 15, 11), ("pz", (2,)), ("pz", (3,)),
+    ("w", 12, 9, 15, 12), ("w", 13, 10, 16, 13), ("w", 14, 11, 17, 14),
+    ("momentum",),
+    ("begin", "n"), ("w", 14, 11, 17, 14), ("w", 15, 12, 18, 15), ("w", 16, 13, 19, 16),
+    ("small", "n", (0,)), ("small", "n", (1,)), ("w", 17, 14, 20, 16), ("small", "n", (2,)), ("w", 18, 14, 21, 16),
+    ("small", "n", (3,)), ("w", 19, 15, 22, 17), ("small", "n", (4,)), ("w", 20, 15, 23, 18), ("small", "n", (5,)),
+    ("w", 21, 16, 24, 19),
+    ("small", "n", (6,)),
+    ("squares",),
+]
+for j in range(8):
+    SCHEDULE += [("lows", j), ("w", 22 + j, 17 + j, 25 + j, 20 + j)]
+SCHEDULE += [("totals",), ("all", 30, 25, 3)]
 
 
 def split(ref, t, tiles, count):
@@ -107,12 +131,11 @@
         self.have = {(q, True, c) for c in range(CHUNKS)}
         self.got = {way: 0 for way in self.into}
         self.put = {way: 0 for way in self.out}
-        self.round = 0
-
-    def fill(self, depth, limit=None):
+
+    def push(self, along, across):
         moves = []
-        for way in ("up", "down", "cross"):
-            while self.put[way] < min(len(self.out[way]), self.round + depth):
+        for way, goal in (("up", along), ("down", along), ("cross", across)):
+            while self.put[way] < min(len(self.out[way]), goal):
                 entry = self.out[way][self.put[way]]
                 if entry not in self.have:
                     break
@@ -120,16 +143,17 @@
                 self.put[way] += 1
         return moves
 
-    def turn(self, lag, depth):
-        moves = self.fill(depth)
-        self.round += 1
-        for way in ("cross", "down", "up"):
-            while self.got[way] < min(len(self.into[way]), self.round - lag):
-                entry = self.into[way][self.got[way]]
-                moves.append(("wait", way, entry))
-                self.have.add(entry)
-                self.got[way] += 1
-                moves += self.fill(depth)
+    def take(self, along, across, push_along, push_across):
+        moves = self.push(push_along, push_across)
+        goals = {"cross": across, "down": along, "up": along}
+        for count in range(1, max(along, across) + 1):
+            for way, goal in goals.items():
+                if self.got[way] < min(len(self.into[way]), goal, count):
+                    entry = self.into[way][self.got[way]]
+                    moves.append(("wait", way, entry))
+                    self.have.add(entry)
+                    self.got[way] += 1
+                    moves += self.push(push_along, push_across)
         return moves
 
     def done(self):
@@ -143,7 +167,7 @@
     x_hbm, q_hbm, k_hbm, v_hbm, c_hbm, mix_hbm, gain_hbm, f_hbm, mom_hbm, w_hbm,
     wall, low, nm_ref, tot_ref,
     x_ref, q_ref, k_ref, v_ref, c_ref, mix_ref, gain_ref, f_ref, mom_ref, w_ref,
-    fall, nmall, fwide, dq, dv, psend, precv, sums,
+    fall, nmall, fwide, dq, dv, psend, precv, pside, pmid, sums,
     l_sem, f_send, f_recv, s_send, s_recv, w_send, w_recv, n_send, n_recv, p_send, p_recv, t_send, t_recv,
 ):
     me = lax.axis_index("fs")
@@ -208,12 +232,8 @@
             device_id={"fs": peer}, device_id_type=MESH,
         )
 
-    def momentum():
+    def momentum(total):
         local["mom"].wait()
-        total = psend[me].astype(jnp.float32)
-        for hop in range(1, n):
-            p_copy(hop).wait_recv()
-            total += precv[hop].astype(jnp.float32)
         length = x_ref.shape[0]
         for t in range(2 * tiles_w):
             m, lanes = t // tiles_w, slice(t % tiles_w * LANES, (t % tiles_w + 1) * LANES)
@@ -306,6 +326,8 @@
         def small_begin(kind, q):
             for i, k in enumerate(reversed(others(q))):
                 small(kind, me, i, index_of(k, True)).start()
+                if kind in DIRECT:
+                    small(kind, me, 4 + i, index_of(k, False)).start()
             small(kind, me, 3, partner).start()
 
         def spread(index, which, to, way):
@@ -314,7 +336,7 @@
         def small_wait(kind, q, k, same):
             index = index_of(k, same)
             small(kind, index, 0, partner).wait_recv()
-            if same:
+            if same and kind not in DIRECT:
                 small(kind, index, 0, partner).start()
             if kind == "f":
                 spread(index, mt, far, 0).start()
@@ -322,6 +344,35 @@
 
         def pieces(q):
             return [(q, False)] + [(k, True) for k in others(q)] + [(k, False) for k in others(q)]
+
+        def place_of(k):
+            return k + flip * (3 - 2 * k)
+
+        def p_order(q):
+            return list(reversed(others(q))) + [q]
+
+        def p_across(index, at):
+            return pltpu.make_async_remote_copy(
+                src_ref=psend.at[index], dst_ref=pside.at[at], send_sem=p_send.at[at], recv_sem=p_recv.at[at],
+                device_id={"fs": partner}, device_id_type=MESH,
+            )
+
+        def p_along(q, k):
+            return pltpu.make_async_remote_copy(
+                src_ref=pmid.at[place_of(k)], dst_ref=precv.at[place], send_sem=p_send.at[4 + place_of(k)],
+                recv_sem=p_recv.at[4 + place], device_id={"fs": index_of(k, True)}, device_id_type=MESH,
+            )
+
+        def gathered():
+            total = psend[me].astype(jnp.float32) + pside[place].astype(jnp.float32)
+            for hop in range(1, 4):
+                at = (place + hop) % 4
+                pltpu.make_async_remote_copy(
+                    src_ref=pmid.at[at], dst_ref=precv.at[at], send_sem=p_send.at[4 + at], recv_sem=p_recv.at[4 + at],
+                    device_id={"fs": partner}, device_id_type=MESH,
+                ).wait_recv()
+                total += precv[at].astype(jnp.float32)
+            return total
 
         def segment(tokens):
             for q in (0, 1):
@@ -331,19 +382,30 @@
                     for token in tokens:
                         kind, *rest = token
                         if kind == "w":
-                            lag, count = rest
-                            for _ in range(count):
-                                run(q, states[q].turn(lag, DEPTH))
+                            run(q, states[q].take(*rest))
                         elif kind == "begin":
                             small_begin(rest[0], q)
-                        elif kind == "fill":
-                            run(q, states[q].fill(rest[0]))
+                        elif kind == "px":
+                            for k in p_order(q):
+                                p_across(index_of(k, False), place_of(k)).start()
+                        elif kind == "pz":
+                            for i in rest[0]:
+                                k = p_order(q)[i]
+                                p_across(index_of(k, True), place_of(k)).wait_recv()
+                                if k != q:
+                                    pmid[place_of(k)] = (
+                                        psend[index_of(k, True)].astype(jnp.float32)
+                                        + pside[place_of(k)].astype(jnp.float32)
+                                    ).astype(pmid.dtype)
+                                    p_along(q, k).start()
                         elif kind == "small":
                             for i in rest[1]:
                                 small_wait(rest[0], q, *pieces(q)[i])
                         elif kind == "all":
+                            along, across, ahead = rest
                             while not states[q].done():
-                                run(q, states[q].turn(*rest, DEPTH))
+                                run(q, states[q].take(along, across, along + ahead, across + ahead))
+                                along, across = along + 1, across + 1
                         elif kind == "spread":
                             for k, same in pieces(q):
                                 index = index_of(k, same)
@@ -358,40 +420,32 @@
                                 for entry in states[q].out[way]:
                                     w_copy(q, way, entry).wait_send()
                             for name in ("f", "n"):
-                                for way in range(4):
+                                for way in range(7 if name in DIRECT else 4):
                                     small(name, me, way, partner).wait_send()
-                                for k in others(q):
+                                for k in () if name in DIRECT else others(q):
                                     small(name, index_of(k, True), 0, partner).wait_send()
+                            for k in range(4):
+                                p_across(index_of(k, False), place_of(k)).wait_send()
+                                if k != q:
+                                    p_along(q, k).wait_send()
                             for k, same in pieces(q):
                                 for way in range(3):
                                     spread(index_of(k, same), mt, near, way).wait_send()
 
+        computes = {
+            "project": project, "squares": squares, "totals": totals, "momentum": lambda: momentum(gathered()),
+            "lows": lambda j: lows(j * deep, deep),
+        }
         head(0)
         pl.semaphore_wait(barrier, n - 1 + tp - 1)
-        segment([("begin", "f"), ("fill", DEPTH)])
-        head(1)
-        segment([("small", "f", (0,)), ("w", 4, 1)])
-        head(2)
-        segment([("small", "f", (1, 2)), ("w", 4, 1)])
-        head(3)
-        for i in range(4, heads):
-            head(i)
-        segment([("w", 4, 1), ("small", "f", (3,)), ("w", 4, 2), ("small", "f", (4, 5, 6)), ("w", 4, 1), ("spread",)])
-        project()
-        for hop in range(1, n):
-            p_copy(hop).start()
-        segment([("w", 4, 8)])
-        momentum()
-        segment([
-            ("begin", "n"), ("w", 4, 2), ("small", "n", (0, 1, 2)), ("w", 4, 2), ("small", "n", (3,)), ("w", 4, 2),
-            ("small", "n", (4, 5, 6)),
-        ])
-        squares()
-        for j in range(n):
-            lows(j * deep, deep)
-            segment([("w", 4, 1)])
-        totals()
-        segment([("all", 4)])
+        for token in SCHEDULE:
+            if token[0] == "head":
+                for i in range(token[1], heads if token[1] == 3 else token[1] + 1):
+                    head(i)
+            elif token[0] in computes:
+                computes[token[0]](*token[1:])
+            else:
+                segment([token])
         segment([("sent",)])
     else:
         for i in range(heads):
@@ -420,7 +474,12 @@
         each(lambda hop: block("f", (me + hop) % n, hop).wait_recv())
         project()
         each(lambda hop: p_copy(hop).start())
-        momentum()
+
+        def add(hop, total):
+            p_copy(hop).wait_recv()
+            return total + precv[hop].astype(jnp.float32)
+
+        momentum(lax.fori_loop(1, n, add, psend[me].astype(jnp.float32)))
         each(lambda hop: block("n", me, hop).start())
         each(lambda hop: block("n", (me + hop) % n, hop).wait_recv())
         squares()
@@ -430,10 +489,9 @@
         each(lambda hop: block("w", (me + hop) % n, hop).wait_recv())
         for kind in ("f", "w", "n"):
             each(lambda hop, kind=kind: block(kind, me, hop).wait_send())
+        each(lambda hop: p_copy(hop).wait_send())
     for hop in range(1, tp):
         t_copy(hop).wait_send()
-    for hop in range(1, n):
-        p_copy(hop).wait_send()
 
 
 def finish(n, entries, wall, low, nm_ref, tot_ref, step_hbm, nm_hbm, copies_hbm, step, copies, sems):
@@ -517,12 +575,14 @@
             pltpu.VMEM((length, cols), jnp.bfloat16),
             pltpu.VMEM((n, 2, rank_here, cols), wire),
             pltpu.VMEM((n, 2, rank_here, cols), wire),
+            pltpu.VMEM((4, 2, rank_here, cols), wire),
+            pltpu.VMEM((4, 2, rank_here, cols), wire),
             pltpu.VMEM((tp, 2, LANES), jnp.float32),
             dma((len(args),)),
             *(
                 (
-                    dma((n, 4)), dma((n,)), dma((n, 3)), dma((n, 3)),
-                    dma((n, CHUNKS, 3)), dma((n, CHUNKS)), dma((n, 4)), dma((n,)),
+                    dma((n, 7)), dma((n,)), dma((n, 3)), dma((n, 3)),
+                    dma((n, CHUNKS, 3)), dma((n, CHUNKS)), dma((n, 7)), dma((n,)),
                 )
                 if n == 8
                 else (dma((n,)), dma((n,)), dma((1,)), dma((1,)), dma((n,)), dma((n,)), dma((n,)), dma((n,)))

time: 85.8 us -> 76 us (0.89)
  Pallas kernels: 85.1 us -> 75.2 us
    pallas_call x1, Pallas kernels: 82.4 us -> 72.6 us  [per_device(): pl.pallas_call(functools.partial(kernel, n, tp, heads), out_shape=(pltpu....]
where the time goes in v2:
time: 76 us; the launch traced here: 75.8 us
  Pallas kernels  75.2 us (99%)
    pallas_call x1, Pallas kernels, per_device(): pl.pallas_call(functools.partial(kernel, n, tp, heads), out_shape=(pltpu....  72.6 us
    pallas_call x1, Pallas kernels, per_device(): pl.pallas_call(functools.partial(finish, n, rank * cols * tp), out_shape=...  2.62 us

profile of v2, /device:TPU:0, one launch (start us, length us, event | category | flops | bytes accessed | tf_op | source)
XLA Modules:
  0.0 75.8 jit_solution(9519840886155067062)
XLA Ops:
  0.6 72.6 %shard_map.121 = (bf16[16384,128]{1,0:T(8,128)(2,1)S(1)}, f32[16384,128]{1,0:T(8,128)S(1)}, f32[256,128]{1,0:T(8,128)S(1)}, f32[2,128]{1,0:T(2,128)S(1)}) custom-call(bf16[384,2048]{1,0:T(8,128)(2,1)} %x_hbm.1, bf16[384,512]{1,0:T(8,128)(2,1)} %q_hbm.1, bf16[384,512]{1,0:T(8,128)(2,1)} %k_hbm.1, bf16[384,512]{1,0:T(8,128)(2,1)} %v_hbm.1, ...), custom_call_target="tpu_custom_call" | custom-call | tf_op jit(solution)/shard_map/pallas_call | solution.py:550
  73.2 2.6 %shard_map.122 = (f32[2048,128]{1,0:T(8,128)}, f32[256,128]{1,0:T(8,128)}, bf16[16384,128]{1,0:T(8,128)(2,1)}) custom-call(bf16[16384,128]{1,0:T(8,128)(2,1)S(1)} %get-tuple-element.10.wall, f32[16384,128]{1,0:T(8,128)S(1)} %get-tuple-element.11.low, f32[256,128]{1,0:T(8,128)S(1)} %get-tuple-element.12.nm_ref, f32[2,128]{1,0:T(2,128)S(1)} %get-tuple-element.13.tot_ref), custom_call_target="tpu_custom_call" | custom-call | tf_op jit(solution)/shard_map/pallas_call | solution.py:598

commit v3 on v2

--- a/solution.py
+++ b/solution.py
@@ -14,10 +14,8 @@
 LANES = 128
 CHUNKS = 8
 WIDE = 2
-DIRECT = ()
 SCHEDULE = [
-    ("begin", "f"), ("w", 0, 0, 4, 2),
-    ("head", 1),
+    ("begin", "f"), ("own",), ("w", 0, 0, 4, 2), ("head", 0), ("head", 1),
     ("small", "f", (0,)), ("w", 0, 0, 5, 2),
     ("head", 2),
     ("small", "f", (1, 2)), ("w", 0, 0, 10, 2),
@@ -200,12 +198,15 @@
     here = pl.ds(pl.multiple_of(me * deep, deep), deep)
     for t in range(2 * tiles_f):
         fall[here, t * LANES : (t + 1) * LANES] = split(fwide, t, tiles_f, deep).astype(jnp.bfloat16)
-    local["w"].wait()
-    wall[pl.ds(pl.multiple_of(me * deep * per_row, 16), deep * per_row), :] = w_ref[...].astype(jnp.bfloat16)
-    for name in ("gain", "mix", "q", "k", "v", "c"):
-        local[name].wait()
+
+    def own_weights():
+        local["w"].wait()
+        wall[pl.ds(pl.multiple_of(me * deep * per_row, 16), deep * per_row), :] = w_ref[...].astype(jnp.bfloat16)
 
     def head(i):
+        if i == 0:
+            for name in ("gain", "mix", "q", "k", "v", "c"):
+                local[name].wait()
         head_step(i, q_ref, k_ref, v_ref, c_ref, mix_ref, gain_ref, dq, dv)
 
     def remote(src, send, recv, axis, target):
@@ -299,7 +300,7 @@
             k, same, chunk = entry
             index = index_of(k, same)
             return remote(
-                weights(index, chunk, CHUNKS), w_send.at[index, chunk, ways[way]], w_recv.at[index, chunk],
+                weights(index, chunk, CHUNKS), w_send.at[ways[way]], w_recv.at[index, chunk],
                 "fs", target(q, way),
             )
 
@@ -318,26 +319,24 @@
         def others(q):
             return sorted((k for k in range(4) if k != q), key=lambda k: (abs(k - q), k))
 
-        def small(kind, index, way, to):
+        def small(kind, index, to):
             if kind == "f":
-                return remote(piece(index, mt), f_send.at[index, way], f_recv.at[index], "fs", to)
-            return remote(nmall.at[index], n_send.at[index, way], n_recv.at[index], "fs", to)
+                return remote(piece(index, mt), f_send.at[0], f_recv.at[index], "fs", to)
+            return remote(nmall.at[index], n_send.at[0], n_recv.at[index], "fs", to)
 
         def small_begin(kind, q):
             for i, k in enumerate(reversed(others(q))):
-                small(kind, me, i, index_of(k, True)).start()
-                if kind in DIRECT:
-                    small(kind, me, 4 + i, index_of(k, False)).start()
-            small(kind, me, 3, partner).start()
+                small(kind, me, index_of(k, True)).start()
+            small(kind, me, partner).start()
 
         def spread(index, which, to, way):
-            return remote(piece(index, which), s_send.at[index, way], s_recv.at[index, way], "tp", to)
+            return remote(piece(index, which), s_send.at[0], s_recv.at[index, way], "tp", to)
 
         def small_wait(kind, q, k, same):
             index = index_of(k, same)
-            small(kind, index, 0, partner).wait_recv()
-            if same and kind not in DIRECT:
-                small(kind, index, 0, partner).start()
+            small(kind, index, partner).wait_recv()
+            if same:
+                small(kind, index, partner).start()
             if kind == "f":
                 spread(index, mt, far, 0).start()
                 spread(index, mt, near, 1).start()
@@ -353,13 +352,13 @@
 
         def p_across(index, at):
             return pltpu.make_async_remote_copy(
-                src_ref=psend.at[index], dst_ref=pside.at[at], send_sem=p_send.at[at], recv_sem=p_recv.at[at],
+                src_ref=psend.at[index], dst_ref=pside.at[at], send_sem=p_send.at[0], recv_sem=p_recv.at[at],
                 device_id={"fs": partner}, device_id_type=MESH,
             )
 
         def p_along(q, k):
             return pltpu.make_async_remote_copy(
-                src_ref=pmid.at[place_of(k)], dst_ref=precv.at[place], send_sem=p_send.at[4 + place_of(k)],
+                src_ref=pmid.at[place_of(k)], dst_ref=precv.at[place], send_sem=p_send.at[1],
                 recv_sem=p_recv.at[4 + place], device_id={"fs": index_of(k, True)}, device_id_type=MESH,
             )
 
@@ -368,7 +367,7 @@
             for hop in range(1, 4):
                 at = (place + hop) % 4
                 pltpu.make_async_remote_copy(
-                    src_ref=pmid.at[at], dst_ref=precv.at[at], send_sem=p_send.at[4 + at], recv_sem=p_recv.at[4 + at],
+                    src_ref=pmid.at[at], dst_ref=precv.at[at], send_sem=p_send.at[1], recv_sem=p_recv.at[4 + at],
                     device_id={"fs": partner}, device_id_type=MESH,
                 ).wait_recv()
                 total += precv[at].astype(jnp.float32)
@@ -417,26 +416,25 @@
                                 spread(index, (near + 2) % tp, near, 2).wait_recv()
                         elif kind == "sent":
                             for way in ways:
-                                for entry in states[q].out[way]:
-                                    w_copy(q, way, entry).wait_send()
-                            for name in ("f", "n"):
-                                for way in range(7 if name in DIRECT else 4):
-                                    small(name, me, way, partner).wait_send()
-                                for k in () if name in DIRECT else others(q):
-                                    small(name, index_of(k, True), 0, partner).wait_send()
-                            for k in range(4):
-                                p_across(index_of(k, False), place_of(k)).wait_send()
-                                if k != q:
-                                    p_along(q, k).wait_send()
-                            for k, same in pieces(q):
-                                for way in range(3):
-                                    spread(index_of(k, same), mt, near, way).wait_send()
+                                if states[q].out[way]:
+                                    all_sent(wall, w_send.at[ways[way]], len(states[q].out[way]), CHUNKS)
+
+        def all_sent(whole, sem, count, per_block):
+            rows = whole.shape[0] // n // per_block * count
+            part = whole.at[pl.ds(0, rows)]
+            remote(part, sem, sem, "fs", partner).wait_send()
+
+        def rest_sent():
+            all_sent(fall, f_send.at[0], 7, tp)
+            all_sent(fall, s_send.at[0], 21, tp)
+            all_sent(nmall, n_send.at[0], 7, 1)
+            all_sent(psend, p_send.at[0], 4, 1)
+            remote(pmid.at[pl.ds(0, 3)], p_send.at[1], p_send.at[1], "fs", partner).wait_send()
 
         computes = {
-            "project": project, "squares": squares, "totals": totals, "momentum": lambda: momentum(gathered()),
+            "own": own_weights, "project": project, "squares": squares, "totals": totals, "momentum": lambda: momentum(gathered()),
             "lows": lambda j: lows(j * deep, deep),
         }
-        head(0)
         pl.semaphore_wait(barrier, n - 1 + tp - 1)
         for token in SCHEDULE:
             if token[0] == "head":
@@ -447,7 +445,9 @@
             else:
                 segment([token])
         segment([("sent",)])
+        rest_sent()
     else:
+        own_weights()
         for i in range(heads):
             head(i)
         pl.semaphore_wait(barrier, n - 1 + tp - 1)
@@ -581,13 +581,12 @@
             dma((len(args),)),
             *(
                 (
-                    dma((n, 7)), dma((n,)), dma((n, 3)), dma((n, 3)),
-                    dma((n, CHUNKS, 3)), dma((n, CHUNKS)), dma((n, 7)), dma((n,)),
+                    dma((1,)), dma((n,)), dma((1,)), dma((n, 3)),
+                    dma((3,)), dma((n, CHUNKS)), dma((1,)), dma((n,)), dma((2,)), dma((n,)),
                 )
                 if n == 8
-                else (dma((n,)), dma((n,)), dma((1,)), dma((1,)), dma((n,)), dma((n,)), dma((n,)), dma((n,)))
+                else (dma((n,)), dma((n,)), dma((1,)), dma((1,)), dma((n,)), dma((n,)), dma((n,)), dma((n,)), dma((n,)), dma((n,)))
             ),
-            dma((n,)), dma((n,)),
             dma((tp,)), dma((tp,)),
         ],
         compiler_params=pltpu.CompilerParams(

time: 76 us -> 72.1 us (0.949)
  Pallas kernels: 75.2 us -> 71.2 us
    pallas_call x1, Pallas kernels: 72.6 us -> 68.6 us  [per_device(): pl.pallas_call(functools.partial(kernel, n, tp, heads), out_shape=(pltpu....]
where the time goes in v3:
time: 72.1 us; the launch traced here: 72 us
  Pallas kernels  71.2 us (99%)
  between operations  0.8 us (1%)
    pallas_call x1, Pallas kernels, per_device(): pl.pallas_call(functools.partial(kernel, n, tp, heads), out_shape=(pltpu....  68.6 us
    pallas_call x1, Pallas kernels, per_device(): pl.pallas_call(functools.partial(finish, n, rank * cols * tp), out_shape=...  2.62 us

profile of v3, /device:TPU:0, one launch (start us, length us, event | category | flops | bytes accessed | tf_op | source)
XLA Modules:
  0.0 72.0 jit_solution(7212574766106617237)
XLA Ops:
  0.6 68.6 %shard_map.121 = (bf16[16384,128]{1,0:T(8,128)(2,1)S(1)}, f32[16384,128]{1,0:T(8,128)S(1)}, f32[256,128]{1,0:T(8,128)S(1)}, f32[2,128]{1,0:T(2,128)S(1)}) custom-call(bf16[384,2048]{1,0:T(8,128)(2,1)} %x_hbm.1, bf16[384,512]{1,0:T(8,128)(2,1)} %q_hbm.1, bf16[384,512]{1,0:T(8,128)(2,1)} %k_hbm.1, bf16[384,512]{1,0:T(8,128)(2,1)} %v_hbm.1, ...), custom_call_target="tpu_custom_call" | custom-call | tf_op jit(solution)/shard_map/pallas_call | solution.py:550
  69.2 2.6 %shard_map.122 = (f32[2048,128]{1,0:T(8,128)}, f32[256,128]{1,0:T(8,128)}, bf16[16384,128]{1,0:T(8,128)(2,1)}) custom-call(bf16[16384,128]{1,0:T(8,128)(2,1)S(1)} %get-tuple-element.10.wall, f32[16384,128]{1,0:T(8,128)S(1)} %get-tuple-element.11.low, f32[256,128]{1,0:T(8,128)S(1)} %get-tuple-element.12.nm_ref, f32[2,128]{1,0:T(2,128)S(1)} %get-tuple-element.13.tot_ref), custom_call_target="tpu_custom_call" | custom-call | tf_op jit(solution)/shard_map/pallas_call | solution.py:597

commit v4 on v3

--- a/solution.py
+++ b/solution.py
@@ -15,28 +15,21 @@
 CHUNKS = 8
 WIDE = 2
 SCHEDULE = [
-    ("begin", "f"), ("own",), ("w", 0, 0, 4, 2), ("head", 0), ("head", 1),
-    ("small", "f", (0,)), ("w", 0, 0, 5, 2),
-    ("head", 2),
-    ("small", "f", (1, 2)), ("w", 0, 0, 10, 2),
-    ("head", 3),
-    ("small", "f", (3,)), ("w", 0, 0, 10, 8), ("small", "f", (4, 5, 6)), ("spread",),
-    ("w", 6, 6, 12, 10),
-    ("project",),
-    ("px",), ("w", 8, 8, 14, 10), ("w", 9, 8, 15, 10),
-    ("pz", (0,)), ("w", 10, 8, 15, 10), ("pz", (1,)), ("w", 11, 8, 15, 11), ("pz", (2,)), ("pz", (3,)),
-    ("w", 12, 9, 15, 12), ("w", 13, 10, 16, 13), ("w", 14, 11, 17, 14),
-    ("momentum",),
-    ("begin", "n"), ("w", 14, 11, 17, 14), ("w", 15, 12, 18, 15), ("w", 16, 13, 19, 16),
-    ("small", "n", (0,)), ("small", "n", (1,)), ("w", 17, 14, 20, 16), ("small", "n", (2,)), ("w", 18, 14, 21, 16),
-    ("small", "n", (3,)), ("w", 19, 15, 22, 17), ("small", "n", (4,)), ("w", 20, 15, 23, 18), ("small", "n", (5,)),
-    ("w", 21, 16, 24, 19),
-    ("small", "n", (6,)),
-    ("squares",),
+    ("begin", "f"), ("own",), ("w", 0, 0, 19, 4), ("small", "f", (0,)), ("small", "f", (3,)), ("small", "f", (1,)),
+    ("head", 0), ("w", 0, 2, 13, 4), ("small", "f", (2,)), ("head", 1), ("small", "f", (4,)), ("w", 0, 2, 14, 2),
+    ("small", "f", (6,)), ("w", 2, 0, 17, 19), ("small", "f", (5,)), ("w", 4, 4, 7, 2), ("head", 2), ("head", 3),
+    ("spread",), ("w", 3, 1, 16, 16), ("project",), ("pb",), ("w", 5, 10, 9, 4), ("w", 1, 1, 15, 6), ("pd", (0,), ()),
+    ("pd", (1,), ()), ("w", 9, 1, 17, 5), ("w", 7, 4, 16, 5), ("w", 15, 5, 16, 19), ("pd", (2,), ()),
+    ("pd", (3,), (0,)), ("pd", (4,), ()), ("w", 5, 3, 16, 1), ("w", 10, 0, 13, 3), ("w", 5, 3, 15, 1),
+    ("pd", (5,), (1,)), ("pd", (6,), ()), ("w", 8, 0, 35, 12), ("pd", (7,), ()), ("w", 7, 1, 32, 13), ("pxs",),
+    ("w", 14, 1, 35, 14), ("w", 3, 5, 39, 25), ("w", 14, 1, 36, 13), ("w", 11, 1, 35, 13), ("pd", (8,), ()),
+    ("pd", (9,), ()), ("pt",), ("w", 1, 1, 40, 27), ("momentum",), ("begin", "n"), ("w", 24, 2, 15, 58),
+    ("w", 24, 2, 16, 58), ("small", "n", (3,)), ("w", 23, 1, 15, 55), ("w", 24, 9, 55, 52), ("w", 22, 2, 55, 59),
+    ("small", "n", (2,)), ("small", "n", (1,)), ("small", "n", (0,)), ("w", 25, 1, 0, 51), ("small", "n", (5,)),
+    ("w", 26, 3, 18, 47), ("small", "n", (6,)), ("w", 26, 5, 18, 46), ("small", "n", (4,)), ("squares",),
+    ("w", 24, 4, 17, 45), ("lows", 0), ("lows", 1), ("lows", 2), ("lows", 3), ("lows", 4), ("lows", 5),
+    ("w", 29, 3, 59, 69), ("lows", 6), ("lows", 7), ("totals",), ("all", 43, 34, 17),
 ]
-for j in range(8):
-    SCHEDULE += [("lows", j), ("w", 22 + j, 17 + j, 25 + j, 20 + j)]
-SCHEDULE += [("totals",), ("all", 30, 25, 3)]
 
 
 def split(ref, t, tiles, count):
@@ -165,7 +158,7 @@
     x_hbm, q_hbm, k_hbm, v_hbm, c_hbm, mix_hbm, gain_hbm, f_hbm, mom_hbm, w_hbm,
     wall, low, nm_ref, tot_ref,
     x_ref, q_ref, k_ref, v_ref, c_ref, mix_ref, gain_ref, f_ref, mom_ref, w_ref,
-    fall, nmall, fwide, dq, dv, psend, precv, pside, pmid, sums,
+    fall, nmall, fwide, dq, dv, psend, precv, pin, pmid, xsend, xrecv, ptot, sums,
     l_sem, f_send, f_recv, s_send, s_recv, w_send, w_recv, n_send, n_recv, p_send, p_recv, t_send, t_recv,
 ):
     me = lax.axis_index("fs")
@@ -347,31 +340,51 @@
         def place_of(k):
             return k + flip * (3 - 2 * k)
 
-        def p_order(q):
-            return list(reversed(others(q))) + [q]
-
-        def p_across(index, at):
+        def p_items(q):
+            if q == 0:
+                return [("down", 0, False), ("down", 0, True)]
+            return [
+                ("up", 3, False), ("up", 3, True), ("up", 2, False), ("down", 0, False), ("up", 2, True),
+                ("down", 0, True), ("up", 1, False), ("down", 1, False), ("up", 1, True), ("down", 1, True),
+            ]
+
+        def p_slot(way, k, same):
+            w = 0 if way == "up" else 1
+            return (w + flip * (1 - 2 * w)) * 8 + place_of(k) * 2 + (0 if same else 1)
+
+        def p_hop(q, way, k, same, src):
+            slot = p_slot(way, k, same)
+            to = min(max(q + (1 if way == "up" else -1), 0), 3)
             return pltpu.make_async_remote_copy(
-                src_ref=psend.at[index], dst_ref=pside.at[at], send_sem=p_send.at[0], recv_sem=p_recv.at[at],
+                src_ref=src, dst_ref=pin.at[slot], send_sem=p_send.at[0], recv_sem=p_recv.at[slot],
+                device_id={"fs": index_of(to, True)}, device_id_type=MESH,
+            )
+
+        def p_pass(q, way, k, same):
+            slot = p_slot(way, k, same)
+            p_hop(1, way, k, same, pin.at[slot]).wait_recv()
+            if k != q:
+                pmid[slot] = (
+                    psend[index_of(k, same)].astype(jnp.float32) + pin[slot].astype(jnp.float32)
+                ).astype(pmid.dtype)
+                p_hop(q, way, k, same, pmid.at[slot]).start()
+
+        def p_sum(q, same):
+            total = psend[me if same else partner].astype(jnp.float32)
+            for way, k, parity_same in p_items(q):
+                if k == q and parity_same == same:
+                    total += pin[p_slot(way, k, same)].astype(jnp.float32)
+            return total
+
+        def p_cross():
+            return pltpu.make_async_remote_copy(
+                src_ref=xsend, dst_ref=xrecv, send_sem=p_send.at[1], recv_sem=p_recv.at[16],
                 device_id={"fs": partner}, device_id_type=MESH,
             )
 
-        def p_along(q, k):
-            return pltpu.make_async_remote_copy(
-                src_ref=pmid.at[place_of(k)], dst_ref=precv.at[place], send_sem=p_send.at[1],
-                recv_sem=p_recv.at[4 + place], device_id={"fs": index_of(k, True)}, device_id_type=MESH,
-            )
-
         def gathered():
-            total = psend[me].astype(jnp.float32) + pside[place].astype(jnp.float32)
-            for hop in range(1, 4):
-                at = (place + hop) % 4
-                pltpu.make_async_remote_copy(
-                    src_ref=pmid.at[at], dst_ref=precv.at[at], send_sem=p_send.at[1], recv_sem=p_recv.at[4 + at],
-                    device_id={"fs": partner}, device_id_type=MESH,
-                ).wait_recv()
-                total += precv[at].astype(jnp.float32)
-            return total
+            p_cross().wait_recv()
+            return ptot[...] + xrecv[...].astype(jnp.float32)
 
         def segment(tokens):
             for q in (0, 1):
@@ -384,19 +397,18 @@
                             run(q, states[q].take(*rest))
                         elif kind == "begin":
                             small_begin(rest[0], q)
-                        elif kind == "px":
-                            for k in p_order(q):
-                                p_across(index_of(k, False), place_of(k)).start()
-                        elif kind == "pz":
-                            for i in rest[0]:
-                                k = p_order(q)[i]
-                                p_across(index_of(k, True), place_of(k)).wait_recv()
-                                if k != q:
-                                    pmid[place_of(k)] = (
-                                        psend[index_of(k, True)].astype(jnp.float32)
-                                        + pside[place_of(k)].astype(jnp.float32)
-                                    ).astype(pmid.dtype)
-                                    p_along(q, k).start()
+                        elif kind == "pb" and q == 0:
+                            for k in (3, 2, 1):
+                                for same in (False, True):
+                                    p_hop(q, "up", k, same, psend.at[index_of(k, same)]).start()
+                        elif kind == "pd":
+                            for i in rest[1 - q]:
+                                p_pass(q, *p_items(q)[i])
+                        elif kind == "pxs":
+                            xsend[...] = p_sum(q, False).astype(xsend.dtype)
+                            p_cross().start()
+                        elif kind == "pt":
+                            ptot[...] = p_sum(q, True)
                         elif kind == "small":
                             for i in rest[1]:
                                 small_wait(rest[0], q, *pieces(q)[i])
@@ -428,8 +440,8 @@
             all_sent(fall, f_send.at[0], 7, tp)
             all_sent(fall, s_send.at[0], 21, tp)
             all_sent(nmall, n_send.at[0], 7, 1)
-            all_sent(psend, p_send.at[0], 4, 1)
-            remote(pmid.at[pl.ds(0, 3)], p_send.at[1], p_send.at[1], "fs", partner).wait_send()
+            remote(pmid.at[pl.ds(0, 6)], p_send.at[0], p_send.at[0], "fs", partner).wait_send()
+            p_cross().wait_send()
 
         computes = {
             "own": own_weights, "project": project, "squares": squares, "totals": totals, "momentum": lambda: momentum(gathered()),
@@ -547,8 +559,24 @@
         inputs, queries, keys, values, head_cot, mixing, head_gain[None, :],
         to_rows(factors), to_rows(moments), to_rows(weights),
     )
+    semaphores = [
+            dma((len(args),)),
+            *(
+                (
+                    dma((1,)), dma((n,)), dma((1,)), dma((n, 3)),
+                    dma((3,)), dma((n, CHUNKS)), dma((1,)), dma((n,)), dma((2,)), dma((17,)),
+                )
+                if n == 8
+                else (dma((n,)), dma((n,)), dma((1,)), dma((1,)), dma((n,)), dma((n,)), dma((n,)), dma((n,)), dma((n,)), dma((n,)))
+            ),
+            dma((tp,)), dma((tp,)),
+    ]
+
+    def scoped(*refs):
+        pl.run_scoped(lambda *sems: kernel(n, tp, heads, *refs, *sems), *semaphores)
+
     held = pl.pallas_call(
-        functools.partial(kernel, n, tp, heads),
+        scoped,
         out_shape=(
             pltpu.VMEM((depth * per_row, LANES), jnp.bfloat16),
             pltpu.VMEM((depth * per_row, LANES), jnp.float32),
@@ -575,19 +603,12 @@
             pltpu.VMEM((length, cols), jnp.bfloat16),
             pltpu.VMEM((n, 2, rank_here, cols), wire),
             pltpu.VMEM((n, 2, rank_here, cols), wire),
-            pltpu.VMEM((4, 2, rank_here, cols), wire),
-            pltpu.VMEM((4, 2, rank_here, cols), wire),
+            pltpu.VMEM((16 if n == 8 else 1, 2, rank_here, cols), wire),
+            pltpu.VMEM((16 if n == 8 else 1, 2, rank_here, cols), wire),
+            pltpu.VMEM((2, rank_here, cols), wire),
+            pltpu.VMEM((2, rank_here, cols), wire),
+            pltpu.VMEM((2, rank_here, cols), jnp.float32),
             pltpu.VMEM((tp, 2, LANES), jnp.float32),
-            dma((len(args),)),
-            *(
-                (
-                    dma((1,)), dma((n,)), dma((1,)), dma((n, 3)),
-                    dma((3,)), dma((n, CHUNKS)), dma((1,)), dma((n,)), dma((2,)), dma((n,)),
-                )
-                if n == 8
-                else (dma((n,)), dma((n,)), dma((1,)), dma((1,)), dma((n,)), dma((n,)), dma((n,)), dma((n,)), dma((n,)), dma((n,)))
-            ),
-            dma((tp,)), dma((tp,)),
         ],
         compiler_params=pltpu.CompilerParams(
             collective_id=0, has_side_effects=True, vmem_limit_bytes=36 * 1024 * 1024

time: 72.1 us -> 66.7 us (0.925)
  Pallas kernels: 71.2 us -> 65.9 us
    pallas_call x1, Pallas kernels: 68.6 us -> 63.3 us  [per_device(): pl.pallas_call(scoped, out_shape=(pltpu.VMEM((depth * per_row, LANES), jn...]
where the time goes in v4:
time: 66.7 us; the launch traced here: 66.5 us
  Pallas kernels  65.9 us (99%)
    pallas_call x1, Pallas kernels, per_device(): pl.pallas_call(scoped, out_shape=(pltpu.VMEM((depth * per_row, LANES), jn...  63.3 us
    pallas_call x1, Pallas kernels, per_device(): pl.pallas_call(functools.partial(finish, n, rank * cols * tp), out_shape=...  2.62 us

profile of v4, /device:TPU:0, one launch (start us, length us, event | category | flops | bytes accessed | tf_op | source)
XLA Modules:
  0.0 66.5 jit_solution(16645501532313918797)
XLA Ops:
  0.6 63.3 %shard_map.121 = (bf16[16384,128]{1,0:T(8,128)(2,1)S(1)}, f32[16384,128]{1,0:T(8,128)S(1)}, f32[256,128]{1,0:T(8,128)S(1)}, f32[2,128]{1,0:T(2,128)S(1)}) custom-call(bf16[384,2048]{1,0:T(8,128)(2,1)} %refs_0_.1, bf16[384,512]{1,0:T(8,128)(2,1)} %refs_1_.1, bf16[384,512]{1,0:T(8,128)(2,1)} %refs_2_.1, bf16[384,512]{1,0:T(8,128)(2,1)} %refs_3_.1, ...), custom_call_target="tpu_custom_call" | custom-call | tf_op jit(solution)/shard_map/pallas_call | solution.py:578
  63.9 2.6 %shard_map.122 = (f32[2048,128]{1,0:T(8,128)}, f32[256,128]{1,0:T(8,128)}, bf16[16384,128]{1,0:T(8,128)(2,1)}) custom-call(bf16[16384,128]{1,0:T(8,128)(2,1)S(1)} %get-tuple-element.10.wall, f32[16384,128]{1,0:T(8,128)S(1)} %get-tuple-element.11.low, f32[256,128]{1,0:T(8,128)S(1)} %get-tuple-element.12.nm_ref, f32[2,128]{1,0:T(2,128)S(1)} %get-tuple-element.13.tot_ref), custom_call_target="tpu_custom_call" | custom-call | tf_op jit(solution)/shard_map/pallas_call | solution.py:618

commit v5 on v4

--- a/solution.py
+++ b/solution.py
@@ -12,23 +12,23 @@
 RATE_BASE = 0.5
 MESH = pl.DeviceIdType.MESH
 LANES = 128
-CHUNKS = 8
-WIDE = 2
+CHUNKS = 16
+WIDE = 3
 SCHEDULE = [
-    ("begin", "f"), ("own",), ("w", 0, 0, 19, 4), ("small", "f", (0,)), ("small", "f", (3,)), ("small", "f", (1,)),
-    ("head", 0), ("w", 0, 2, 13, 4), ("small", "f", (2,)), ("head", 1), ("small", "f", (4,)), ("w", 0, 2, 14, 2),
-    ("small", "f", (6,)), ("w", 2, 0, 17, 19), ("small", "f", (5,)), ("w", 4, 4, 7, 2), ("head", 2), ("head", 3),
-    ("spread",), ("w", 3, 1, 16, 16), ("project",), ("pb",), ("w", 5, 10, 9, 4), ("w", 1, 1, 15, 6), ("pd", (0,), ()),
-    ("pd", (1,), ()), ("w", 9, 1, 17, 5), ("w", 7, 4, 16, 5), ("w", 15, 5, 16, 19), ("pd", (2,), ()),
-    ("pd", (3,), (0,)), ("pd", (4,), ()), ("w", 5, 3, 16, 1), ("w", 10, 0, 13, 3), ("w", 5, 3, 15, 1),
-    ("pd", (5,), (1,)), ("pd", (6,), ()), ("w", 8, 0, 35, 12), ("pd", (7,), ()), ("w", 7, 1, 32, 13), ("pxs",),
-    ("w", 14, 1, 35, 14), ("w", 3, 5, 39, 25), ("w", 14, 1, 36, 13), ("w", 11, 1, 35, 13), ("pd", (8,), ()),
-    ("pd", (9,), ()), ("pt",), ("w", 1, 1, 40, 27), ("momentum",), ("begin", "n"), ("w", 24, 2, 15, 58),
-    ("w", 24, 2, 16, 58), ("small", "n", (3,)), ("w", 23, 1, 15, 55), ("w", 24, 9, 55, 52), ("w", 22, 2, 55, 59),
-    ("small", "n", (2,)), ("small", "n", (1,)), ("small", "n", (0,)), ("w", 25, 1, 0, 51), ("small", "n", (5,)),
-    ("w", 26, 3, 18, 47), ("small", "n", (6,)), ("w", 26, 5, 18, 46), ("small", "n", (4,)), ("squares",),
-    ("w", 24, 4, 17, 45), ("lows", 0), ("lows", 1), ("lows", 2), ("lows", 3), ("lows", 4), ("lows", 5),
-    ("w", 29, 3, 59, 69), ("lows", 6), ("lows", 7), ("totals",), ("all", 43, 34, 17),
+    ("begin", "f"), ("own",), ("w", 0, 0, 93, 9), ("small", "f", (0,)), ("small", "f", (3,)), ("small", "f", (1,)),
+    ("small", "f", (2,)), ("head", 0), ("w", 1, 0, 92, 4), ("w", 0, 0, 92, 4), ("w", 0, 0, 75, 10),
+    ("w", 0, 2, 77, 14), ("w", 1, 2, 74, 16), ("head", 1), ("w", 2, 2, 77, 17), ("small", "f", (6,)), ("head", 2),
+    ("w", 0, 9, 45, 67), ("small", "f", (4,)), ("head", 3), ("small", "f", (5,)), ("w", 7, 10, 42, 60),
+    ("w", 9, 0, 52, 0), ("spread",), ("project",), ("w", 7, 5, 42, 57), ("pb",), ("pd", (0,), ()), ("pd", (1,), ()),
+    ("w", 2, 2, 53, 59), ("w", 16, 6, 31, 53), ("w", 28, 7, 29, 44), ("pd", (2,), ()), ("pd", (3,), (0,)),
+    ("w", 0, 11, 25, 24), ("pd", (4,), ()), ("pd", (5,), (1,)), ("w", 22, 33, 43, 46), ("pd", (6,), ()),
+    ("pd", (7,), ()), ("pxs",), ("pd", (8,), ()), ("pd", (9,), ()), ("pt",), ("w", 24, 30, 35, 59),
+    ("w", 22, 17, 63, 39), ("w", 23, 38, 64, 47), ("w", 16, 32, 55, 43), ("w", 19, 27, 65, 49), ("momentum",),
+    ("begin", "n"), ("w", 46, 26, 33, 95), ("small", "n", (0,)), ("small", "n", (3,)), ("w", 19, 46, 71, 37),
+    ("small", "n", (2,)), ("small", "n", (1,)), ("w", 51, 32, 20, 53), ("w", 52, 23, 24, 67), ("small", "n", (5,)),
+    ("small", "n", (4,)), ("small", "n", (6,)), ("squares",), ("w", 41, 35, 22, 57), ("lows", 0), ("lows", 1),
+    ("lows", 2), ("w", 39, 31, 41, 52), ("lows", 3), ("w", 53, 30, 24, 52), ("w", 54, 23, 21, 48), ("lows", 4),
+    ("lows", 5), ("w", 55, 23, 21, 48), ("lows", 6), ("lows", 7), ("totals",), ("all", 117, 122, 81),
 ]
 
 
@@ -514,20 +514,24 @@
     nm_copy.start()
     rate = RATE_BASE / jnp.sqrt(1.0 + tot_ref[...] / entries)
     count = min(rows // 16, 1024)
-    odd = lax.broadcasted_iota(jnp.int32, (count, LANES), 0) % 2 == 1
-    rates = jnp.where(odd, rate[1:2], rate[0:1])
+    odd = lax.broadcasted_iota(jnp.int32, (8, LANES), 0) % 2 == 1
+    rates = jnp.where(odd, rate[1:2], rate[0:1])[None]
     started = [nm_copy]
-    for i in range(0, own, min(count, own)):
-        size = min(count, own)
-        start = pl.multiple_of(me * own + i, 8)
-        step[i : i + size, :] = low[pl.ds(start, size), :] * rates[:size]
-    started.append(pltpu.make_async_copy(step, step_hbm, sems.at[1]))
-    started[-1].start()
+
+    def scaled(start, size):
+        return (low[pl.ds(start, size), :].reshape(size // 8, 8, LANES) * rates).reshape(size, LANES)
+
     for i in range(rows // count):
         at = slice(i * count, (i + 1) * count)
-        copies[at, :] = (wall[at, :].astype(jnp.float32) - low[at, :] * rates).astype(jnp.bfloat16)
+        copies[at, :] = (wall[at, :].astype(jnp.float32) - scaled(i * count, count)).astype(jnp.bfloat16)
         started.append(pltpu.make_async_copy(copies.at[at], copies_hbm.at[at], sems.at[2 + i]))
         started[-1].start()
+        if i == 1:
+            for first in range(0, own, min(count, own)):
+                size = min(count, own)
+                step[first : first + size, :] = scaled(pl.multiple_of(me * own + first, 8), size)
+            started.append(pltpu.make_async_copy(step, step_hbm, sems.at[1]))
+            started[-1].start()
     for copy in started:
         copy.wait()
 

time: 66.7 us -> 66.4 us (level)
  no operation moved by 1% of the time
where the time goes in v5:
time: 66.4 us; the launch traced here: 66.2 us
  Pallas kernels  65.4 us (98%)
  between operations  0.8 us (1%)
    pallas_call x1, Pallas kernels, per_device(): pl.pallas_call(scoped, out_shape=(pltpu.VMEM((depth * per_row, LANES), jn...  62.9 us
    pallas_call x1, Pallas kernels, per_device(): pl.pallas_call(functools.partial(finish, n, rank * cols * tp), out_shape=...  2.55 us

profile of v5, /device:TPU:0, one launch (start us, length us, event | category | flops | bytes accessed | tf_op | source)
XLA Modules:
  0.0 66.2 jit_solution(14411970700190302679)
XLA Ops:
  0.6 62.9 %shard_map.121 = (bf16[16384,128]{1,0:T(8,128)(2,1)S(1)}, f32[16384,128]{1,0:T(8,128)S(1)}, f32[256,128]{1,0:T(8,128)S(1)}, f32[2,128]{1,0:T(2,128)S(1)}) custom-call(bf16[384,2048]{1,0:T(8,128)(2,1)} %refs_0_.1, bf16[384,512]{1,0:T(8,128)(2,1)} %refs_1_.1, bf16[384,512]{1,0:T(8,128)(2,1)} %refs_2_.1, bf16[384,512]{1,0:T(8,128)(2,1)} %refs_3_.1, ...), custom_call_target="tpu_custom_call" | custom-call | tf_op jit(solution)/shard_map/pallas_call | solution.py:582
  63.5 2.6 %shard_map.122 = (f32[2048,128]{1,0:T(8,128)}, f32[256,128]{1,0:T(8,128)}, bf16[16384,128]{1,0:T(8,128)(2,1)}) custom-call(bf16[16384,128]{1,0:T(8,128)(2,1)S(1)} %get-tuple-element.10.wall, f32[16384,128]{1,0:T(8,128)S(1)} %get-tuple-element.11.low, f32[256,128]{1,0:T(8,128)S(1)} %get-tuple-element.12.nm_ref, f32[2,128]{1,0:T(2,128)S(1)} %get-tuple-element.13.tot_ref), custom_call_target="tpu_custom_call" | custom-call | tf_op jit(solution)/shard_map/pallas_call | solution.py:622

commit v6 on v5

--- a/solution.py
+++ b/solution.py
@@ -445,7 +445,7 @@
 
         computes = {
             "own": own_weights, "project": project, "squares": squares, "totals": totals, "momentum": lambda: momentum(gathered()),
-            "lows": lambda j: lows(j * deep, deep),
+            "lows": lambda j: lows(j * deep, 4 * deep) if j % 4 == 0 else None,
         }
         pl.semaphore_wait(barrier, n - 1 + tp - 1)
         for token in SCHEDULE:

time: 66.4 us -> 66.4 us (level)
  no operation moved by 1% of the time
where the time goes in v6:
time: 66.4 us; the launch traced here: 66.2 us
  Pallas kernels  65.4 us (98%)
  between operations  0.8 us (1%)
    pallas_call x1, Pallas kernels, per_device(): pl.pallas_call(scoped, out_shape=(pltpu.VMEM((depth * per_row, LANES), jn...  62.9 us
    pallas_call x1, Pallas kernels, per_device(): pl.pallas_call(functools.partial(finish, n, rank * cols * tp), out_shape=...  2.55 us

profile of v6, /device:TPU:0, one launch (start us, length us, event | category | flops | bytes accessed | tf_op | source)
XLA Modules:
  0.0 66.2 jit_solution(14058105610495820597)
XLA Ops:
  0.6 62.9 %shard_map.121 = (bf16[16384,128]{1,0:T(8,128)(2,1)S(1)}, f32[16384,128]{1,0:T(8,128)S(1)}, f32[256,128]{1,0:T(8,128)S(1)}, f32[2,128]{1,0:T(2,128)S(1)}) custom-call(bf16[384,2048]{1,0:T(8,128)(2,1)} %refs_0_.1, bf16[384,512]{1,0:T(8,128)(2,1)} %refs_1_.1, bf16[384,512]{1,0:T(8,128)(2,1)} %refs_2_.1, bf16[384,512]{1,0:T(8,128)(2,1)} %refs_3_.1, ...), custom_call_target="tpu_custom_call" | custom-call | tf_op jit(solution)/shard_map/pallas_call | solution.py:582
  63.5 2.6 %shard_map.122 = (f32[2048,128]{1,0:T(8,128)}, f32[256,128]{1,0:T(8,128)}, bf16[16384,128]{1,0:T(8,128)(2,1)}) custom-call(bf16[16384,128]{1,0:T(8,128)(2,1)S(1)} %get-tuple-element.10.wall, f32[16384,128]{1,0:T(8,128)S(1)} %get-tuple-element.11.low, f32[256,128]{1,0:T(8,128)S(1)} %get-tuple-element.12.nm_ref, f32[2,128]{1,0:T(2,128)S(1)} %get-tuple-element.13.tot_ref), custom_call_target="tpu_custom_call" | custom-call | tf_op jit(solution)/shard_map/pallas_call | solution.py:622
